TPU v7x, 32 devices: a whole 2x2x4 slice. The times are simulated.
32 devices in a mesh: ep: 8 (over z, y), tp: 4 (over x, core).
Axes of the slice: x: 2, y: 2, z: 4, core: 2. Of those that a mesh axis runs over, the one named last changes fastest.
Arguments:
- queries: bfloat16 [4096, 1536], P('ep', 'tp'), may hold values from -6 to 6
- keys: bfloat16 [4096, 1536], P('ep', 'tp'), may hold values from -6 to 6
- values: bfloat16 [4096, 1536], P('ep', 'tp'), may hold values from -6 to 6
- decay_gate_logits: float32 [4096, 12], P('ep', 'tp'), may hold values from -6 to 6
- correction_logits: bfloat16 [4096, 12], P('ep', 'tp'), may hold values from -6 to 6
- head_decay_speed: float32 [12], P('tp'), may hold values from 0 to 1
- position_log_decay: float32 [4096, 12], P('ep', 'tp'), may hold values from -1 to 0
- head_output_gain: float32 [128], replicated, may hold values from 0.1 to 1.9
- mixer_output_weight: bfloat16 [1536, 2048], P('tp'), may hold values from -0.15625 to 0.15625
- expert_input_tokens: bfloat16 [4096, 2048], P(('ep', 'tp')), may hold values from -6 to 6
- expert_norm_gain: float32 [2048], replicated, may hold values from 0.1 to 1.9
- routes: int32 [4096, 2], P(('ep', 'tp')), may hold values from 0 to 7, all different within a row; in each aligned block of 128 rows (0 to 127, 128 to 255, ...) at most 48 rows name the same one
- chosen_expert_weight: float32 [4096, 2], P(('ep', 'tp')), may hold values from 0.25 to 2.5
- routed_gate_weight: bfloat16 [8, 2048, 1024], P('ep', None, 'tp'), may hold values from -0.125 to 0.125
- routed_up_weight: bfloat16 [8, 2048, 1024], P('ep', None, 'tp'), may hold values from -0.125 to 0.125
- routed_down_weight: bfloat16 [8, 1024, 2048], P('ep', 'tp'), may hold values from -0.1875 to 0.1875
- common_gate_weight: bfloat16 [2048, 1024], P(None, 'tp'), may hold values from -0.125 to 0.125
- common_up_weight: bfloat16 [2048, 1024], P(None, 'tp'), may hold values from -0.125 to 0.125
- common_down_weight: bfloat16 [1024, 2048], P('tp'), may hold values from -0.1875 to 0.1875
Outputs:
- mixer_out: bfloat16 [4096, 2048], P(('ep', 'tp'))
- moe_out: bfloat16 [4096, 2048], P(('ep', 'tp'))
Inputs may be any that keep to these rules, and one draw needn't show every extreme that they name: `routes`: each row names 2 different experts; the rows of one device name no expert more than 48 times, and some device names some expert exactly 48 times.
All inputs are finite; a program needn't handle non-finite values.
Results may differ from a plain program's by a relative error of at most 0.017.
Values may be sent and summed in bfloat16 or wider, within the bound.
A program may use at most 128 MiB of HBM per device.

v0:
```python
import functools

import jax
import jax.numpy as jnp
from jax import lax
from jax.experimental import pallas as pl
from jax.experimental.pallas import tpu as pltpu
from jax.sharding import PartitionSpec as P


EPS = 1e-06


SPAN = 64


def halves(x):
    high = x.astype(jnp.bfloat16)
    return high, (x - high.astype(jnp.float32)).astype(jnp.bfloat16)


def product(left, right, numbers):
    left_high, left_low = halves(left)
    right_high, right_low = halves(right)

    def dot(x, y):
        return lax.dot_general(x, y, numbers, preferred_element_type=jnp.float32)

    return dot(left_high, right_high) + (dot(left_high, right_low) + dot(left_low, right_high))


def bmm(left, right, dims):
    return product(left, right, (dims, ((0,), (0,))))


def mm(left, right):
    return product(left, right, (((1,), (0,)), ((), ())))


def unit_lower_inverse(lower, rows, cols):
    inverse = jnp.where(rows == cols, 1.0, 0.0) - jnp.where(
        ((rows >> 1) == (cols >> 1)), lower, 0.0
    )
    level = 1
    while (1 << level) < SPAN:
        below = ((rows >> (level + 1)) == (cols >> (level + 1))) & (
            (rows >> level) != (cols >> level)
        )
        part = jnp.where(below, lower, 0.0)
        inverse = inverse - bmm(bmm(inverse, part, ((2,), (1,))), inverse, ((2,), (1,)))
        level += 1
    return inverse


def local_kernel(q_ref, k_ref, v_ref, ccol_ref, crow_ref, bcol_ref, g_ref, z_ref, total_ref):
    width = q_ref.shape[1]
    count = q_ref.shape[0] // SPAN
    shape = (count, SPAN, width)
    q = q_ref[...].astype(jnp.float32)
    k = k_ref[...].astype(jnp.float32)
    v = v_ref[...].astype(jnp.float32).reshape(shape)
    q = q * lax.rsqrt(jnp.sum(q * q, axis=-1, keepdims=True) + EPS) * width ** (-0.5)
    k = k * lax.rsqrt(jnp.sum(k * k, axis=-1, keepdims=True) + EPS)
    q = q.reshape(shape)
    k = k.reshape(shape)
    ccol = ccol_ref[0].reshape(count, SPAN, 1)
    crow = crow_ref[0]
    bcol = bcol_ref[0].reshape(count, SPAN, 1)
    rows = lax.broadcasted_iota(jnp.int32, (count, SPAN, SPAN), 1)
    cols = lax.broadcasted_iota(jnp.int32, (count, SPAN, SPAN), 2)
    decay = jnp.exp(jnp.where(rows >= cols, ccol - crow, -jnp.inf))
    keyed = k * bcol
    lower = jnp.where(rows > cols, bmm(keyed, k, ((2,), (2,))) * decay, 0.0)
    inverse = unit_lower_inverse(lower, rows, cols)
    grown = jnp.exp(ccol)
    solved = bmm(
        inverse, jnp.concatenate([keyed * grown, v * bcol], axis=-1), ((2,), (1,))
    )
    scores = bmm(q, k, ((2,), (2,))) * decay
    q_scaled = q * grown
    last = ccol[:, SPAN - 1 :, :]
    carried = k * jnp.exp(last - ccol)
    mixed = bmm(scores, solved, ((2,), (1,)))
    readout = q_scaled - mixed[:, :, :width]
    eye_r = lax.broadcasted_iota(jnp.int32, (width, width), 0)
    eye_c = lax.broadcasted_iota(jnp.int32, (width, width), 1)
    eye = jnp.where(eye_r == eye_c, 1.0, 0.0)
    state = jnp.concatenate([eye, jnp.zeros_like(eye)], axis=1)
    for n in range(count):
        seen = mm(readout[n], state)
        g_ref[0, n * SPAN : (n + 1) * SPAN, :] = seen[:, :width]
        z_ref[0, n * SPAN : (n + 1) * SPAN, :] = seen[:, width:] + mixed[n][:, width:]
        both = mm(carried[n].T, solved[n])
        trans = jnp.exp(last[n]) * eye - both[:, :width]
        state = mm(trans, state)
        state = jnp.concatenate([state[:, :width], state[:, width:] + both[:, width:]], axis=1)
    total_ref[0] = state.astype(jnp.bfloat16)


def finish_kernel(place_ref, gathered_ref, g_ref, z_ref, gain_ref, out_ref):
    width = g_ref.shape[2]

    def one(turn, state):
        both = gathered_ref[turn, 0].astype(jnp.float32)
        return mm(both[:, :width], state) + both[:, width:]

    state = lax.fori_loop(0, place_ref[0], one, jnp.zeros((width, width), jnp.float32))
    out = mm(g_ref[0], state) + z_ref[0]
    out = out * lax.rsqrt(jnp.mean(out * out, axis=-1, keepdims=True) + EPS) * gain_ref[...]
    out_ref[...] = out.astype(jnp.bfloat16)


def token_mixer_heads(
    queries,
    keys,
    values,
    decay_gate_logits,
    correction_logits,
    head_decay_speed,
    position_log_decay,
    head_output_gain,
):
    heads = decay_gate_logits.shape[1]
    length = queries.shape[0]
    width = queries.shape[1] // heads
    count = length // SPAN
    log_gate = -head_decay_speed * jax.nn.softplus(decay_gate_logits) + position_log_decay
    log_gate = log_gate.T.reshape(heads, count, SPAN)
    at = jnp.arange(SPAN)
    cum = jnp.sum(
        jnp.where(at[:, None] >= at[None, :], log_gate[:, :, None, :], 0.0), axis=-1
    )
    beta = jax.nn.sigmoid(correction_logits.astype(jnp.float32)).T.reshape(heads, length, 1)
    by_head = pl.BlockSpec((length, width), lambda h: (0, h))
    column = pl.BlockSpec((1, length, 1), lambda h: (h, 0, 0))
    whole = pl.BlockSpec((1, length, width), lambda h: (h, 0, 0))
    local_call = pl.pallas_call(
        local_kernel,
        grid=(heads,),
        in_specs=[
            by_head,
            by_head,
            by_head,
            column,
            pl.BlockSpec((1, count, 1, SPAN), lambda h: (h, 0, 0, 0)),
            column,
        ],
        out_specs=[whole, whole, pl.BlockSpec((1, width, 2 * width), lambda h: (h, 0, 0))],
        out_shape=[
            jax.ShapeDtypeStruct((heads, length, width), jnp.float32),
            jax.ShapeDtypeStruct((heads, length, width), jnp.float32),
            jax.ShapeDtypeStruct((heads, width, 2 * width), jnp.bfloat16),
        ],
        cost_estimate=pl.CostEstimate(
            flops=3_000_000_000, bytes_accessed=4_000_000, transcendentals=200_000
        ),
    )
    readout, local_out, total = local_call(
        queries,
        keys,
        values,
        cum.reshape(heads, length, 1),
        cum.reshape(heads, count, 1, SPAN),
        beta,
    )
    gathered = lax.all_gather(total, "ep")
    place = lax.axis_index("ep").astype(jnp.int32).reshape(1)
    devices = gathered.shape[0]
    return pl.pallas_call(
        finish_kernel,
        grid=(heads,),
        in_specs=[
            pl.BlockSpec(memory_space=pltpu.SMEM),
            pl.BlockSpec((devices, 1, width, 2 * width), lambda h: (0, h, 0, 0)),
            whole,
            whole,
            pl.BlockSpec((1, width), lambda h: (0, 0)),
        ],
        out_specs=by_head,
        out_shape=jax.ShapeDtypeStruct((length, heads * width), jnp.bfloat16),
        cost_estimate=pl.CostEstimate(
            flops=500_000_000, bytes_accessed=4_000_000, transcendentals=2_000
        ),
    )(place, gathered, readout, local_out, head_output_gain.reshape(1, width))


def norm_rows(expert_input_tokens, expert_norm_gain):
    rows_f = expert_input_tokens.astype(jnp.float32)
    scaled = (
        rows_f
        * lax.rsqrt(jnp.mean(rows_f * rows_f, axis=-1, keepdims=True) + EPS)
        * expert_norm_gain
    )
    return scaled.astype(jnp.bfloat16)


def gated_hidden(rows_in, w_gate, w_up):
    gate_val = jnp.dot(rows_in, w_gate, preferred_element_type=jnp.float32)
    up_val = jnp.dot(rows_in, w_up, preferred_element_type=jnp.float32)
    return (jax.nn.silu(gate_val) * up_val).astype(jnp.bfloat16)


def slot_layout(routes, capacity):
    flat = routes.reshape(-1)
    at = jnp.arange(flat.shape[0], dtype=jnp.int32)
    same = (flat[:, None] == flat[None, :]) & (at[None, :] < at[:, None])
    before = jnp.sum(same.astype(jnp.int32), axis=1)
    return (flat * capacity + before).reshape(routes.shape)


def plain_shards(
    queries,
    keys,
    values,
    decay_gate_logits,
    correction_logits,
    head_decay_speed,
    position_log_decay,
    head_output_gain,
    mixer_output_weight,
    expert_input_tokens,
    expert_norm_gain,
    routes,
    chosen_expert_weight,
    routed_gate_weight,
    routed_up_weight,
    routed_down_weight,
    common_gate_weight,
    common_up_weight,
    common_down_weight,
):
    normed = token_mixer_heads(
        queries,
        keys,
        values,
        decay_gate_logits,
        correction_logits,
        head_decay_speed,
        position_log_decay,
        head_output_gain,
    )
    mixer_out = lax.psum_scatter(
        jnp.dot(normed, mixer_output_weight, preferred_element_type=jnp.float32).astype(
            jnp.bfloat16
        ),
        "tp",
        scatter_dimension=0,
        tiled=True,
    )
    normed_in = norm_rows(expert_input_tokens, expert_norm_gain)
    tokens_own, top_k = routes.shape
    model_width = expert_input_tokens.shape[1]
    experts = lax.axis_size("ep")
    capacity = 3 * tokens_own * top_k // (2 * experts)
    slot_count = experts * capacity
    slots = slot_layout(routes, capacity)
    numbers = jnp.arange(slot_count, dtype=jnp.int32)
    sends = sum(
        (slots[None, :, k] == numbers[:, None]).astype(jnp.bfloat16) for k in range(top_k)
    )
    outgoing = jnp.dot(sends, normed_in, preferred_element_type=jnp.float32).astype(
        jnp.bfloat16
    )
    arrived = lax.all_to_all(
        outgoing.reshape(experts, capacity, model_width),
        "ep",
        split_axis=0,
        concat_axis=0,
        tiled=True,
    ).reshape(slot_count, model_width)
    gate_all = lax.all_gather(routed_gate_weight[0], "tp")
    up_all = lax.all_gather(routed_up_weight[0], "tp")
    down_all = lax.all_gather(routed_down_weight[0], "tp", axis=0, tiled=True)
    hidden = jnp.concatenate(
        [gated_hidden(arrived, gate_all[t], up_all[t]) for t in range(gate_all.shape[0])],
        axis=1,
    )
    slot_sums = jnp.dot(hidden, down_all, preferred_element_type=jnp.float32).astype(
        jnp.bfloat16
    )
    returned = lax.all_to_all(
        slot_sums.reshape(experts, capacity, model_width),
        "ep",
        split_axis=0,
        concat_axis=0,
        tiled=True,
    ).reshape(slot_count, model_width)
    shared_hidden = gated_hidden(
        lax.all_gather(normed_in, "tp", axis=0, tiled=True), common_gate_weight, common_up_weight
    )
    shared = lax.psum_scatter(
        jnp.dot(shared_hidden, common_down_weight, preferred_element_type=jnp.float32).astype(
            jnp.bfloat16
        ),
        "tp",
        scatter_dimension=0,
        tiled=True,
    ).astype(jnp.float32)
    weights = sum(
        jnp.where(
            slots[:, k : k + 1] == numbers[None, :], chosen_expert_weight[:, k : k + 1], 0.0
        )
        for k in range(top_k)
    )
    coarse = weights.astype(jnp.bfloat16)
    fine = (weights - coarse.astype(jnp.float32)).astype(jnp.bfloat16)
    routed = jnp.dot(coarse, returned, preferred_element_type=jnp.float32) + jnp.dot(
        fine, returned, preferred_element_type=jnp.float32
    )
    moe_out = (shared + routed).astype(jnp.bfloat16)
    return (mixer_out, moe_out)


MESH = pl.DeviceIdType.MESH
CUTS = 4
OWN, CORE, CROSS, FAR = range(4)


def scaled_rows(rows, gain):
    rows_f = rows.astype(jnp.float32)
    norm = lax.rsqrt(jnp.mean(rows_f * rows_f, axis=-1, keepdims=True) + EPS)
    return (rows_f * norm * gain).astype(jnp.bfloat16)


def silu_product(gate_val, up_val):
    return (gate_val / (1.0 + jnp.exp(-gate_val)) * up_val).astype(jnp.bfloat16)


def fused_kernel(
    devices,
    q_ref,
    k_ref,
    v_ref,
    decay_ref,
    correct_ref,
    speed_ref,
    log_ref,
    head_gain_ref,
    tok_ref,
    gain_ref,
    sends_ref,
    coarse_ref,
    fine_ref,
    mixw_hbm,
    rg_hbm,
    ru_hbm,
    rd_hbm,
    cg_hbm,
    cu_hbm,
    cd_hbm,
    mix_ref,
    moe_ref,
    wg,
    wu,
    wd,
    cg,
    cu,
    cd,
    mw,
    toks,
    outgoing,
    arrived,
    hid,
    slot_out,
    returned,
    sh_part,
    sh_in,
    sh_cross,
    sh_far,
    mx_part,
    mx_in,
    mx_cross,
    mx_far,
    ccol_s,
    crow_s,
    bcol_s,
    gs,
    zs,
    tot,
    tot_bf,
    pair_in,
    pair_tot,
    s_in,
    s_out,
    state_s,
    normed,
    local_sem,
    w_send,
    w_recv,
    d_send,
    d_recv,
    r_send,
    r_recv,
    r_local,
    rs_send,
    rs_recv,
    c_send,
    c_recv,
):
    e = lax.axis_index("ep")
    t = lax.axis_index("tp")
    heads = decay_ref.shape[1]
    width = q_ref.shape[1] // heads
    length = q_ref.shape[0]
    count = length // SPAN
    tokens, model = tok_ref.shape
    capacity = arrived.shape[1]
    slots = devices * capacity
    unit = wg.shape[2]
    cut = model // CUTS
    core_t = t + 1 - 2 * (t % 2)
    core = (e, core_t)
    cross = (e, (t + 2) % 4)

    def remote(src, dst, send, recv, peer):
        return pltpu.make_async_remote_copy(
            src_ref=src,
            dst_ref=dst,
            send_sem=send,
            recv_sem=recv,
            device_id=peer,
            device_id_type=MESH,
        )

    barrier = pltpu.get_barrier_semaphore()
    for o in range(1, devices):
        pl.semaphore_signal(
            barrier, inc=1, device_id=((e + o) % devices, t), device_id_type=MESH
        )
    for o in range(1, 4):
        pl.semaphore_signal(barrier, inc=1, device_id=(e, (t + o) % 4), device_id_type=MESH)
    pl.semaphore_wait(barrier, devices + 2)

    def cols(j):
        return pl.ds(pl.multiple_of(j * cut, cut), cut)

    def spread(i, src, place):
        remote(src, place(CROSS), w_send.at[i, 0], w_recv.at[i, 0], cross).start()
        remote(src, place(CORE), w_send.at[i, 1], w_recv.at[i, 1], core).start()

    def forward(i, place):
        remote(place(CROSS), place(CROSS), w_send.at[i, 0], w_recv.at[i, 0], cross).wait_recv()
        remote(place(CROSS), place(FAR), w_send.at[i, 2], w_recv.at[i, 2], core).start()

    def take(i, place):
        remote(place(CORE), place(CORE), w_send.at[i, 1], w_recv.at[i, 1], core).wait_recv()
        remote(place(FAR), place(FAR), w_send.at[i, 2], w_recv.at[i, 2], core).wait_recv()

    def sent(i, place):
        remote(place(CROSS), place(CROSS), w_send.at[i, 0], w_recv.at[i, 0], cross).wait_send()
        remote(place(CORE), place(CORE), w_send.at[i, 1], w_recv.at[i, 1], core).wait_send()
        remote(place(FAR), place(FAR), w_send.at[i, 2], w_recv.at[i, 2], core).wait_send()

    def tok_at(r):
        return toks.at[r]

    def gate_at(r):
        return wg.at[r]

    def up_at(r):
        return wu.at[r]

    def down_at(j):
        return lambda r: wd.at[r, :, cols(j)]

    spread(0, tok_ref, tok_at)
    spread(1, rg_hbm, gate_at)
    spread(2, ru_hbm, up_at)
    for j in range(CUTS):
        remote(
            rd_hbm.at[:, cols(j)], wd.at[CROSS, :, cols(j)], w_send.at[3 + j, 0], w_recv.at[3 + j, 0], cross
        ).start()
        remote(
            rd_hbm.at[:, cols(j)], wd.at[CORE, :, cols(j)], w_send.at[3 + j, 1], w_recv.at[3 + j, 1], core
        ).start()

    locals_ = [
        pltpu.make_async_copy(src, dst, local_sem.at[n])
        for n, (src, dst) in enumerate(
            (
                (cg_hbm, cg),
                (cu_hbm, cu),
                (cd_hbm, cd),
                (rg_hbm, wg.at[OWN]),
                (ru_hbm, wu.at[OWN]),
                (rd_hbm, wd.at[OWN]),
                (mixw_hbm, mw),
            )
        )
    ]
    for copy in locals_:
        copy.start()

    toks[OWN] = scaled_rows(tok_ref[...], gain_ref[...])
    outgoing[...] = (
        jnp.dot(sends_ref[...], toks[OWN], preferred_element_type=jnp.float32)
        .astype(jnp.bfloat16)
        .reshape(outgoing.shape)
    )

    softplus = jnp.maximum(decay_ref[...], 0.0) + jnp.log1p(jnp.exp(-jnp.abs(decay_ref[...])))
    log_gate = -speed_ref[...] * softplus + log_ref[...]
    beta = 1.0 / (1.0 + jnp.exp(-correct_ref[...].astype(jnp.float32)))
    rows = lax.broadcasted_iota(jnp.int32, (count, SPAN, SPAN), 1)
    cols_at = lax.broadcasted_iota(jnp.int32, (count, SPAN, SPAN), 2)
    for h in range(heads):
        one = log_gate[:, h : h + 1].reshape(count, SPAN, 1)
        crow = jnp.sum(jnp.where(rows <= cols_at, one, 0.0), axis=1, keepdims=True)
        crow_s[h] = crow
        ccol_s[h] = jnp.sum(jnp.where(rows == cols_at, crow, 0.0), axis=2, keepdims=True)
        bcol_s[h] = beta[:, h : h + 1].reshape(count, SPAN, 1)

    for o in range(1, devices):
        peer = (e + o) % devices
        remote(
            outgoing.at[peer], arrived.at[e], d_send.at[o - 1], d_recv.at[o - 1], (peer, t)
        ).start()
    own_rows = pltpu.make_async_copy(outgoing.at[e], arrived.at[e], local_sem.at[7])
    own_rows.start()

    def local_head(h, carry):
        at = pl.ds(pl.multiple_of(h * width, width), width)
        shape = (count, SPAN, width)
        q = q_ref[:, at].astype(jnp.float32)
        k = k_ref[:, at].astype(jnp.float32)
        v = v_ref[:, at].astype(jnp.float32).reshape(shape)
        q = q * lax.rsqrt(jnp.sum(q * q, axis=-1, keepdims=True) + EPS) * width ** (-0.5)
        k = k * lax.rsqrt(jnp.sum(k * k, axis=-1, keepdims=True) + EPS)
        q = q.reshape(shape)
        k = k.reshape(shape)
        ccol = ccol_s[h]
        crow = crow_s[h]
        bcol = bcol_s[h]
        decay = jnp.exp(jnp.where(rows >= cols_at, ccol - crow, -jnp.inf))
        keyed = k * bcol
        lower = jnp.where(rows > cols_at, bmm(keyed, k, ((2,), (2,))) * decay, 0.0)
        inverse = unit_lower_inverse(lower, rows, cols_at)
        grown = jnp.exp(ccol)
        solved = bmm(
            inverse, jnp.concatenate([keyed * grown, v * bcol], axis=-1), ((2,), (1,))
        )
        scores = bmm(q, k, ((2,), (2,))) * decay
        q_scaled = q * grown
        last = ccol[:, SPAN - 1 :, :]
        carried = k * jnp.exp(last - ccol)
        mixed = bmm(scores, solved, ((2,), (1,)))
        readout = q_scaled - mixed[:, :, :width]
        eye_r = lax.broadcasted_iota(jnp.int32, (width, width), 0)
        eye_c = lax.broadcasted_iota(jnp.int32, (width, width), 1)
        eye = jnp.where(eye_r == eye_c, 1.0, 0.0)
        state = jnp.concatenate([eye, jnp.zeros_like(eye)], axis=1)
        for n in range(count):
            seen = mm(readout[n], state)
            gs[h, n * SPAN : (n + 1) * SPAN, :] = seen[:, :width]
            zs[h, n * SPAN : (n + 1) * SPAN, :] = seen[:, width:] + mixed[n][:, width:]
            both = mm(carried[n].T, solved[n])
            trans = jnp.exp(last[n]) * eye - both[:, :width]
            state = mm(trans, state)
            state = jnp.concatenate([state[:, :width], state[:, width:] + both[:, width:]], axis=1)
        tot[h] = state
        tot_bf[h] = state.astype(jnp.bfloat16)
        return carry

    lax.fori_loop(0, heads, local_head, 0)

    odd = e % 2
    pair = e // 2
    pairs = devices // 2
    forward(0, tok_at)
    to_odd = remote(tot_bf, pair_in, c_send.at[0], c_recv.at[0], ((e + 1) % devices, t))

    @pl.when(odd == 0)
    def _():
        to_odd.start()

    take(0, tok_at)
    for n in range(3):
        locals_[n].wait()
    gain = gain_ref[...]
    for r in (CORE, CROSS, FAR):
        if r == CROSS:
            remote(tok_at(FAR), tok_at(FAR), w_send.at[0, 2], w_recv.at[0, 2], core).wait_send()
        toks[r] = scaled_rows(toks[r], gain)
    x_all = toks[...].reshape(4 * tokens, model)
    sh_hid = silu_product(
        jnp.dot(x_all, cg[...], preferred_element_type=jnp.float32),
        jnp.dot(x_all, cu[...], preferred_element_type=jnp.float32),
    )
    sh_part[...] = (
        jnp.dot(sh_hid, cd[...], preferred_element_type=jnp.float32)
        .astype(jnp.bfloat16)
        .reshape(sh_part.shape)
    )

    def reduce_start(n, part, inbox):
        for i, r in enumerate((FAR, CORE)):
            remote(
                part.at[r], inbox.at[1 - i], rs_send.at[n, i], rs_recv.at[n, i], core
            ).start()

    def reduce_cross(n, part, inbox, out, far):
        remote(part.at[FAR], inbox.at[1], rs_send.at[n, 0], rs_recv.at[n, 0], core).wait_recv()
        out[...] = (part[CROSS].astype(jnp.float32) + inbox[1].astype(jnp.float32)).astype(
            jnp.bfloat16
        )
        remote(out, far, rs_send.at[n, 2], rs_recv.at[n, 2], cross).start()

    def reduce_finish(n, part, inbox, out, far):
        remote(part.at[CORE], inbox.at[0], rs_send.at[n, 1], rs_recv.at[n, 1], core).wait_recv()
        remote(out, far, rs_send.at[n, 2], rs_recv.at[n, 2], cross).wait_recv()
        return (
            part[OWN].astype(jnp.float32)
            + inbox[0].astype(jnp.float32)
            + far[...].astype(jnp.float32)
        )

    def reduce_sent(n, part, inbox, out, far):
        remote(part.at[FAR], inbox.at[1], rs_send.at[n, 0], rs_recv.at[n, 0], core).wait_send()
        remote(part.at[CORE], inbox.at[0], rs_send.at[n, 1], rs_recv.at[n, 1], core).wait_send()
        remote(out, far, rs_send.at[n, 2], rs_recv.at[n, 2], cross).wait_send()

    reduce_start(0, sh_part, sh_in)

    @pl.when(odd == 1)
    def _():
        remote(tot_bf, pair_in, c_send.at[0], c_recv.at[0], ((e + 1) % devices, t)).wait_recv()
        for h in range(heads):
            both = mm(tot[h][:, :width], pair_in[h].astype(jnp.float32))
            pair_tot[h, :, :width] = both[:, :width]
            pair_tot[h, :, width:] = both[:, width:] + tot[h][:, width:]

    reduce_cross(0, sh_part, sh_in, sh_cross, sh_far)

    forward(1, gate_at)
    for n in range(3, 6):
        locals_[n].wait()
    for i in (1, 2):
        remote(
            wg.at[CORE], wg.at[CORE], w_send.at[i, 1], w_recv.at[i, 1], core
        ).wait_recv()
    own_rows.wait()
    for o in range(1, devices):
        remote(
            outgoing.at[e], arrived.at[e], d_send.at[o - 1], d_recv.at[o - 1], (e, core_t)
        ).wait_recv()

    def hidden_of(r, carry):
        rows_in = arrived[...].reshape(slots, model)
        hid[r] = silu_product(
            jnp.dot(rows_in, wg[r], preferred_element_type=jnp.float32),
            jnp.dot(rows_in, wu[r], preferred_element_type=jnp.float32),
        )
        return carry

    lax.fori_loop(OWN, CORE + 1, hidden_of, 0)

    next_odd = (e + 2) % devices
    next_even = (e + 1) % devices

    @pl.when(pair > 0)
    def _():
        remote(s_out, s_in, c_send.at[1], c_recv.at[1], (next_odd, t)).wait_recv()

    @pl.when(pair == 0)
    def _():
        s_in[...] = jnp.zeros_like(s_in)

    @pl.when(jnp.logical_and(odd == 1, pair < pairs - 1))
    def _():
        for h in range(heads):
            s_out[h] = (
                mm(pair_tot[h][:, :width], s_in[h].astype(jnp.float32)) + pair_tot[h][:, width:]
            ).astype(jnp.bfloat16)
        remote(s_out, s_in, c_send.at[1], c_recv.at[1], (next_odd, t)).start()
        remote(s_out, s_in, c_send.at[2], c_recv.at[1], (next_even, t)).start()

    @pl.when(odd == 1)
    def _():
        for h in range(heads):
            state_s[h] = mm(
                pair_in[h][:, :width].astype(jnp.float32), s_in[h].astype(jnp.float32)
            ) + pair_in[h][:, width:].astype(jnp.float32)

    @pl.when(odd == 0)
    def _():
        state_s[...] = s_in[...].astype(jnp.float32)

    for h in range(heads):
        out = mm(gs[h], state_s[h]) + zs[h]
        out = out * lax.rsqrt(jnp.mean(out * out, axis=-1, keepdims=True) + EPS)
        normed[:, h * width : (h + 1) * width] = (out * head_gain_ref[...]).astype(jnp.bfloat16)
    locals_[6].wait()
    for r, owner in enumerate((t, core_t, (t + 2) % 4, (core_t + 2) % 4)):
        mine = pl.ds(pl.multiple_of(owner * tokens, tokens), tokens)
        mx_part[r] = jnp.dot(
            normed[mine, :], mw[...], preferred_element_type=jnp.float32
        ).astype(jnp.bfloat16)
    reduce_start(1, mx_part, mx_in)
    forward(2, up_at)
    reduce_cross(1, mx_part, mx_in, mx_cross, mx_far)

    for i in (1, 2):
        remote(wg.at[FAR], wg.at[FAR], w_send.at[i, 2], w_recv.at[i, 2], core).wait_recv()
    lax.fori_loop(CROSS, FAR + 1, hidden_of, 0)

    def down_of(j, carry):
        place = down_at(j)
        forward(3 + j, place)
        take(3 + j, place)
        hidden = jnp.concatenate([hid[r] for r in range(4)], axis=1)
        weight = wd[:, :, cols(j)].reshape(4 * unit, cut)
        slot_out[:, :, cols(j)] = (
            jnp.dot(hidden, weight, preferred_element_type=jnp.float32)
            .astype(jnp.bfloat16)
            .reshape(devices, capacity, cut)
        )
        for o in range(1, devices):
            peer = (e + o) % devices
            remote(
                slot_out.at[peer, :, cols(j)],
                returned.at[e, :, cols(j)],
                r_send.at[j, o - 1],
                r_recv.at[j, o - 1],
                (peer, t),
            ).start()
        pltpu.make_async_copy(
            slot_out.at[e, :, cols(j)], returned.at[e, :, cols(j)], r_local.at[j]
        ).start()
        return carry

    lax.fori_loop(0, CUTS, down_of, 0)

    mix_ref[...] = reduce_finish(1, mx_part, mx_in, mx_cross, mx_far).astype(jnp.bfloat16)
    shared = reduce_finish(0, sh_part, sh_in, sh_cross, sh_far)

    for j in range(CUTS):
        for o in range(1, devices):
            remote(
                slot_out.at[e, :, cols(j)],
                returned.at[e, :, cols(j)],
                r_send.at[j, o - 1],
                r_recv.at[j, o - 1],
                (e, core_t),
            ).wait_recv()
        pltpu.make_async_copy(
            slot_out.at[e, :, cols(j)], returned.at[e, :, cols(j)], r_local.at[j]
        ).wait()
        back = returned[:, :, j * cut : (j + 1) * cut].reshape(slots, cut)
        routed = jnp.dot(coarse_ref[...], back, preferred_element_type=jnp.float32) + jnp.dot(
            fine_ref[...], back, preferred_element_type=jnp.float32
        )
        moe_ref[:, j * cut : (j + 1) * cut] = (
            shared[:, j * cut : (j + 1) * cut] + routed
        ).astype(jnp.bfloat16)

    remote(toks.at[CROSS], toks.at[CROSS], w_send.at[0, 0], w_recv.at[0, 0], cross).wait_send()
    remote(toks.at[CORE], toks.at[CORE], w_send.at[0, 1], w_recv.at[0, 1], core).wait_send()
    sent(1, gate_at)
    sent(2, up_at)
    for j in range(CUTS):
        sent(3 + j, down_at(j))
    for o in range(1, devices):
        remote(
            outgoing.at[e], arrived.at[e], d_send.at[o - 1], d_recv.at[o - 1], (e, core_t)
        ).wait_send()
        for j in range(CUTS):
            remote(
                slot_out.at[e, :, cols(j)],
                returned.at[e, :, cols(j)],
                r_send.at[j, o - 1],
                r_recv.at[j, o - 1],
                (e, core_t),
            ).wait_send()
    reduce_sent(0, sh_part, sh_in, sh_cross, sh_far)
    reduce_sent(1, mx_part, mx_in, mx_cross, mx_far)

    @pl.when(odd == 0)
    def _():
        to_odd.wait_send()

    @pl.when(jnp.logical_and(odd == 1, pair < pairs - 1))
    def _():
        remote(s_out, s_in, c_send.at[1], c_recv.at[1], (next_odd, t)).wait_send()
        remote(s_out, s_in, c_send.at[2], c_recv.at[1], (next_even, t)).wait_send()


def fused_shards(
    queries,
    keys,
    values,
    decay_gate_logits,
    correction_logits,
    head_decay_speed,
    position_log_decay,
    head_output_gain,
    mixer_output_weight,
    expert_input_tokens,
    expert_norm_gain,
    routes,
    chosen_expert_weight,
    routed_gate_weight,
    routed_up_weight,
    routed_down_weight,
    common_gate_weight,
    common_up_weight,
    common_down_weight,
):
    devices = lax.axis_size("ep")
    tokens, top_k = routes.shape
    model = expert_input_tokens.shape[1]
    length = queries.shape[0]
    heads = decay_gate_logits.shape[1]
    width = queries.shape[1] // heads
    count = length // SPAN
    unit = routed_gate_weight.shape[2]
    shared_unit = common_gate_weight.shape[1]
    capacity = 3 * tokens * top_k // (2 * devices)
    slot_count = devices * capacity
    slots = slot_layout(routes, capacity)
    numbers = jnp.arange(slot_count, dtype=jnp.int32)
    sends = sum(
        (slots[None, :, k] == numbers[:, None]).astype(jnp.bfloat16) for k in range(top_k)
    )
    weights = sum(
        jnp.where(
            slots[:, k : k + 1] == numbers[None, :], chosen_expert_weight[:, k : k + 1], 0.0
        )
        for k in range(top_k)
    )
    coarse = weights.astype(jnp.bfloat16)
    fine = (weights - coarse.astype(jnp.float32)).astype(jnp.bfloat16)
    bf, f32 = jnp.bfloat16, jnp.float32
    vmem = pl.BlockSpec(memory_space=pltpu.VMEM)
    anywhere = pl.BlockSpec(memory_space=pl.ANY)
    dma = pltpu.SemaphoreType.DMA
    quarter = (4, tokens, model)
    slot_shape = (devices, capacity, model)
    return pl.pallas_call(
        functools.partial(fused_kernel, devices),
        in_specs=[vmem] * 13 + [anywhere] * 7,
        out_specs=[vmem, vmem],
        out_shape=[jax.ShapeDtypeStruct((tokens, model), bf)] * 2,
        scratch_shapes=[
            pltpu.VMEM((4, model, unit), bf),
            pltpu.VMEM((4, model, unit), bf),
            pltpu.VMEM((4, unit, model), bf),
            pltpu.VMEM((model, shared_unit), bf),
            pltpu.VMEM((model, shared_unit), bf),
            pltpu.VMEM((shared_unit, model), bf),
            pltpu.VMEM(mixer_output_weight.shape, bf),
            pltpu.VMEM(quarter, bf),
            pltpu.VMEM(slot_shape, bf),
            pltpu.VMEM(slot_shape, bf),
            pltpu.VMEM((4, slot_count, unit), bf),
            pltpu.VMEM(slot_shape, bf),
            pltpu.VMEM(slot_shape, bf),
            pltpu.VMEM(quarter, bf),
            pltpu.VMEM((2, tokens, model), bf),
            pltpu.VMEM((tokens, model), bf),
            pltpu.VMEM((tokens, model), bf),
            pltpu.VMEM(quarter, bf),
            pltpu.VMEM((2, tokens, model), bf),
            pltpu.VMEM((tokens, model), bf),
            pltpu.VMEM((tokens, model), bf),
            pltpu.VMEM((heads, count, SPAN, 1), f32),
            pltpu.VMEM((heads, count, 1, SPAN), f32),
            pltpu.VMEM((heads, count, SPAN, 1), f32),
            pltpu.VMEM((heads, length, width), f32),
            pltpu.VMEM((heads, length, width), f32),
            pltpu.VMEM((heads, width, 2 * width), f32),
            pltpu.VMEM((heads, width, 2 * width), bf),
            pltpu.VMEM((heads, width, 2 * width), bf),
            pltpu.VMEM((heads, width, 2 * width), f32),
            pltpu.VMEM((heads, width, width), bf),
            pltpu.VMEM((heads, width, width), bf),
            pltpu.VMEM((heads, width, width), f32),
            pltpu.VMEM((length, heads * width), bf),
            dma((8,)),
            dma((3 + CUTS, 3)),
            dma((3 + CUTS, 3)),
            dma((devices - 1,)),
            dma((devices - 1,)),
            dma((CUTS, devices - 1)),
            dma((CUTS, devices - 1)),
            dma((CUTS,)),
            dma((2, 3)),
            dma((2, 3)),
            dma((3,)),
            dma((2,)),
        ],
        compiler_params=pltpu.CompilerParams(
            collective_id=0, has_side_effects=True, vmem_limit_bytes=62 << 20
        ),
    )(
        queries,
        keys,
        values,
        decay_gate_logits,
        correction_logits,
        head_decay_speed.reshape(1, heads),
        position_log_decay,
        head_output_gain.reshape(1, width),
        expert_input_tokens,
        expert_norm_gain.reshape(1, model),
        sends,
        coarse,
        fine,
        mixer_output_weight,
        routed_gate_weight[0],
        routed_up_weight[0],
        routed_down_weight[0],
        common_gate_weight,
        common_up_weight,
        common_down_weight,
    )


def shards(*args):
    devices, members = lax.axis_size("ep"), lax.axis_size("tp")
    routes, tokens = args[11], args[9]
    capacity = 3 * routes.shape[0] * routes.shape[1] // (2 * devices)
    whole_tiles = capacity % 16 == 0 and tokens.shape[1] % (128 * CUTS) == 0
    if members == 4 and devices % 2 == 0 and whole_tiles:
        return fused_shards(*args)
    return plain_shards(*args)


def solution(mesh):
    return jax.shard_map(
        shards,
        mesh=mesh,
        in_specs=(
            P("ep", "tp"),
            P("ep", "tp"),
            P("ep", "tp"),
            P("ep", "tp"),
            P("ep", "tp"),
            P("tp"),
            P("ep", "tp"),
            P(),
            P("tp", None),
            P(("ep", "tp"), None),
            P(),
            P(("ep", "tp"), None),
            P(("ep", "tp"), None),
            P("ep", None, "tp"),
            P("ep", None, "tp"),
            P("ep", "tp", None),
            P(None, "tp"),
            P(None, "tp"),
            P("tp", None),
        ),
        out_specs=(P(("ep", "tp"), None), P(("ep", "tp"), None)),
        check_vma=False,
    )
```

profile of v0, /device:TPU:0, one launch (start us, length us, event | category | flops | bytes accessed | tf_op | source)
XLA Modules:
  0.0 128.2 jit_solution(18195461970203979874)
XLA Ops:
  0.6 0.8 slice_bitcast_fusion.1
  1.4 0.8 copy.42
  2.2 0.1 eq.71
  2.3 0.2 convert_reduce_fusion
  2.5 0.1 reduce_sum.12
  2.6 0.1 copy.43
  2.7 0.7 multiply_add_fusion
  3.4 0.7 fusion.4.sends_ref
  4.1 1.5 %copy.45.correct_ref = bf16[512,3]{1,0:T(8,128)(2,1)} copy(bf16[512,3]{0,1:T(4,128)(2,1)} %param.23) | data formatting | bytes 6144 | tf_op args[4]
  5.6 0.8 subtract_convert_fusion
  6.4 1.5 %copy.44.decay_ref = f32[512,3]{1,0:T(8,128)} copy(f32[512,3]{0,1:T(4,128)} %param.22) | data formatting | bytes 12288 | tf_op args[3]
  8.0 1.5 %copy.46.log_ref = f32[512,3]{1,0:T(8,128)} copy(f32[512,3]{0,1:T(4,128)} %param.25) | data formatting | bytes 12288 | tf_op args[6]
  9.5 114.9 %shard_map.194 = (bf16[128,2048]{1,0:T(8,128)(2,1)}, bf16[128,2048]{1,0:T(8,128)(2,1)}) custom-call(bf16[512,384]{1,0:T(8,128)(2,1)} %q_ref.1, bf16[512,384]{1,0:T(8,128)(2,1)} %k_ref.1, bf16[512,384]{1,0:T(8,128)(2,1)} %v_ref.1, f32[512,3]{1,0:T(8,128)} %copy.44.decay_ref, bf16[512,3]{1,0:T(8,128)(2,1)} %copy.45.correct_ref, f32[1,3]{1,0:T(1,128)} %bitcast.18, ...), custom_call_target="tpu_custom_call" | custom-call | tf_op jit(solution)/shard_map/pallas_call | solution.py:838
  124.5 1.9 %copy.49 = bf16[128,2048]{1,0:T(8,128)(2,1)} copy(bf16[128,2048]{1,0:T(8,128)(2,1)} %get-tuple-element.10) | data formatting | bytes 1048576
  126.3 1.9 %copy.50 = bf16[128,2048]{1,0:T(8,128)(2,1)} copy(bf16[128,2048]{1,0:T(8,128)(2,1)} %get-tuple-element.11) | data formatting | bytes 1048576
  (1 shorter events, 0.0 us)
where the time goes:
time: 129 us; the launch traced here: 128 us
  Pallas kernels  115 us (89%)
  local copies, waits for them, and re-layouts  10.2 us (8%)
  other arithmetic  2.39 us (2%)
    pallas_call x1, Pallas kernels, fused_shards(): pl.pallas_call(functools.partial(fused_kernel, devices), in_specs=[vmem]...  115 us
    unnamed x6, local copies, waits for them, and re-layouts  9.13 us

commit v1 on v0

--- a/solution.py
+++ b/solution.py
@@ -328,19 +328,18 @@
 
 def fused_kernel(
     devices,
-    q_ref,
-    k_ref,
-    v_ref,
     decay_ref,
     correct_ref,
     speed_ref,
     log_ref,
     head_gain_ref,
-    tok_ref,
     gain_ref,
-    sends_ref,
-    coarse_ref,
-    fine_ref,
+    routes_ref,
+    chosen_ref,
+    q_hbm,
+    k_hbm,
+    v_hbm,
+    tok_hbm,
     mixw_hbm,
     rg_hbm,
     ru_hbm,
@@ -357,6 +356,14 @@
     cu,
     cd,
     mw,
+    q_ref,
+    k_ref,
+    v_ref,
+    tok_ref,
+    hits_ref,
+    weight_ref,
+    lrow_s,
+    brow_s,
     toks,
     outgoing,
     arrived,
@@ -399,11 +406,12 @@
 ):
     e = lax.axis_index("ep")
     t = lax.axis_index("tp")
-    heads = decay_ref.shape[1]
+    heads = decay_ref.shape[0]
     width = q_ref.shape[1] // heads
     length = q_ref.shape[0]
     count = length // SPAN
     tokens, model = tok_ref.shape
+    top_k = routes_ref.shape[0]
     capacity = arrived.shape[1]
     slots = devices * capacity
     unit = wg.shape[2]
@@ -422,58 +430,12 @@
             device_id_type=MESH,
         )
 
-    barrier = pltpu.get_barrier_semaphore()
-    for o in range(1, devices):
-        pl.semaphore_signal(
-            barrier, inc=1, device_id=((e + o) % devices, t), device_id_type=MESH
-        )
-    for o in range(1, 4):
-        pl.semaphore_signal(barrier, inc=1, device_id=(e, (t + o) % 4), device_id_type=MESH)
-    pl.semaphore_wait(barrier, devices + 2)
-
-    def cols(j):
-        return pl.ds(pl.multiple_of(j * cut, cut), cut)
-
-    def spread(i, src, place):
-        remote(src, place(CROSS), w_send.at[i, 0], w_recv.at[i, 0], cross).start()
-        remote(src, place(CORE), w_send.at[i, 1], w_recv.at[i, 1], core).start()
-
-    def forward(i, place):
-        remote(place(CROSS), place(CROSS), w_send.at[i, 0], w_recv.at[i, 0], cross).wait_recv()
-        remote(place(CROSS), place(FAR), w_send.at[i, 2], w_recv.at[i, 2], core).start()
-
-    def take(i, place):
-        remote(place(CORE), place(CORE), w_send.at[i, 1], w_recv.at[i, 1], core).wait_recv()
-        remote(place(FAR), place(FAR), w_send.at[i, 2], w_recv.at[i, 2], core).wait_recv()
-
-    def sent(i, place):
-        remote(place(CROSS), place(CROSS), w_send.at[i, 0], w_recv.at[i, 0], cross).wait_send()
-        remote(place(CORE), place(CORE), w_send.at[i, 1], w_recv.at[i, 1], core).wait_send()
-        remote(place(FAR), place(FAR), w_send.at[i, 2], w_recv.at[i, 2], core).wait_send()
-
-    def tok_at(r):
-        return toks.at[r]
-
-    def gate_at(r):
-        return wg.at[r]
-
-    def up_at(r):
-        return wu.at[r]
-
-    def down_at(j):
-        return lambda r: wd.at[r, :, cols(j)]
-
-    spread(0, tok_ref, tok_at)
-    spread(1, rg_hbm, gate_at)
-    spread(2, ru_hbm, up_at)
-    for j in range(CUTS):
-        remote(
-            rd_hbm.at[:, cols(j)], wd.at[CROSS, :, cols(j)], w_send.at[3 + j, 0], w_recv.at[3 + j, 0], cross
-        ).start()
-        remote(
-            rd_hbm.at[:, cols(j)], wd.at[CORE, :, cols(j)], w_send.at[3 + j, 1], w_recv.at[3 + j, 1], core
-        ).start()
-
+    early = [
+        pltpu.make_async_copy(src, dst, local_sem.at[8 + n])
+        for n, (src, dst) in enumerate(
+            ((tok_hbm, tok_ref), (q_hbm, q_ref), (k_hbm, k_ref), (v_hbm, v_ref))
+        )
+    ]
     locals_ = [
         pltpu.make_async_copy(src, dst, local_sem.at[n])
         for n, (src, dst) in enumerate(
@@ -488,27 +450,116 @@
             )
         )
     ]
+    for copy in early:
+        copy.start()
+
+    barrier = pltpu.get_barrier_semaphore()
+    for o in range(1, devices):
+        pl.semaphore_signal(
+            barrier, inc=1, device_id=((e + o) % devices, t), device_id_type=MESH
+        )
+    for o in range(1, 4):
+        pl.semaphore_signal(barrier, inc=1, device_id=(e, (t + o) % 4), device_id_type=MESH)
+
+    expert = lax.broadcasted_iota(jnp.int32, (devices, tokens), 0)
+    earlier = lax.broadcasted_iota(jnp.int32, (tokens, tokens), 0)
+    earlier = jnp.where(
+        earlier < lax.broadcasted_iota(jnp.int32, (tokens, tokens), 1), 1.0, 0.0
+    ).astype(jnp.bfloat16)
+    number = lax.broadcasted_iota(jnp.int32, (slots, tokens), 0).astype(jnp.float32)
+    base = jnp.zeros((devices, 1), jnp.float32)
+    sends = jnp.zeros((slots, tokens), jnp.bfloat16)
+    token_a = lax.broadcasted_iota(jnp.int32, (tokens, tokens), 0)
+    token_b = lax.broadcasted_iota(jnp.int32, (tokens, tokens), 1)
+    for n in range(top_k):
+        route = routes_ref[n : n + 1, :]
+        chosen = jnp.where(expert == route, 1.0, 0.0)
+        before = base + jnp.dot(
+            chosen.astype(jnp.bfloat16), earlier, preferred_element_type=jnp.float32
+        )
+        base = base + jnp.sum(chosen, axis=1, keepdims=True)
+        slot = route.astype(jnp.float32) * capacity + jnp.sum(
+            chosen * before, axis=0, keepdims=True
+        )
+        hit = jnp.where(number == slot, 1.0, 0.0).astype(jnp.bfloat16)
+        sends = sends + hit
+        hits_ref[n] = hit
+        weight_ref[n] = jnp.sum(
+            jnp.where(token_a == token_b, chosen_ref[n : n + 1, :], 0.0), axis=1, keepdims=True
+        )
+
+    pl.semaphore_wait(barrier, devices + 2)
+
+    def cols(j):
+        return pl.ds(pl.multiple_of(j * cut, cut), cut)
+
+    def spread(i, src, place):
+        remote(src, place(CROSS), w_send.at[i, 0], w_recv.at[i, 0], cross).start()
+        remote(src, place(CORE), w_send.at[i, 1], w_recv.at[i, 1], core).start()
+
+    def forward(i, place):
+        remote(place(CROSS), place(CROSS), w_send.at[i, 0], w_recv.at[i, 0], cross).wait_recv()
+        remote(place(CROSS), place(FAR), w_send.at[i, 2], w_recv.at[i, 2], core).start()
+
+    def take(i, place):
+        remote(place(CORE), place(CORE), w_send.at[i, 1], w_recv.at[i, 1], core).wait_recv()
+        remote(place(FAR), place(FAR), w_send.at[i, 2], w_recv.at[i, 2], core).wait_recv()
+
+    def sent(i, place):
+        remote(place(CROSS), place(CROSS), w_send.at[i, 0], w_recv.at[i, 0], cross).wait_send()
+        remote(place(CORE), place(CORE), w_send.at[i, 1], w_recv.at[i, 1], core).wait_send()
+        remote(place(FAR), place(FAR), w_send.at[i, 2], w_recv.at[i, 2], core).wait_send()
+
+    def tok_at(r):
+        return toks.at[r]
+
+    def gate_at(r):
+        return wg.at[r]
+
+    def up_at(r):
+        return wu.at[r]
+
+    def down_at(j):
+        return lambda r: wd.at[r, :, cols(j)]
+
+    spread(0, tok_hbm, tok_at)
+    spread(1, rg_hbm, gate_at)
+    spread(2, ru_hbm, up_at)
+    for j in range(CUTS):
+        remote(
+            rd_hbm.at[:, cols(j)], wd.at[CROSS, :, cols(j)], w_send.at[3 + j, 0], w_recv.at[3 + j, 0], cross
+        ).start()
+        remote(
+            rd_hbm.at[:, cols(j)], wd.at[CORE, :, cols(j)], w_send.at[3 + j, 1], w_recv.at[3 + j, 1], core
+        ).start()
+
     for copy in locals_:
         copy.start()
 
+    early[0].wait()
     toks[OWN] = scaled_rows(tok_ref[...], gain_ref[...])
     outgoing[...] = (
-        jnp.dot(sends_ref[...], toks[OWN], preferred_element_type=jnp.float32)
+        jnp.dot(sends, toks[OWN], preferred_element_type=jnp.float32)
         .astype(jnp.bfloat16)
         .reshape(outgoing.shape)
     )
 
-    softplus = jnp.maximum(decay_ref[...], 0.0) + jnp.log1p(jnp.exp(-jnp.abs(decay_ref[...])))
-    log_gate = -speed_ref[...] * softplus + log_ref[...]
-    beta = 1.0 / (1.0 + jnp.exp(-correct_ref[...].astype(jnp.float32)))
     rows = lax.broadcasted_iota(jnp.int32, (count, SPAN, SPAN), 1)
     cols_at = lax.broadcasted_iota(jnp.int32, (count, SPAN, SPAN), 2)
     for h in range(heads):
-        one = log_gate[:, h : h + 1].reshape(count, SPAN, 1)
-        crow = jnp.sum(jnp.where(rows <= cols_at, one, 0.0), axis=1, keepdims=True)
-        crow_s[h] = crow
-        ccol_s[h] = jnp.sum(jnp.where(rows == cols_at, crow, 0.0), axis=2, keepdims=True)
-        bcol_s[h] = beta[:, h : h + 1].reshape(count, SPAN, 1)
+        logit = decay_ref[h : h + 1, :]
+        softplus = jnp.maximum(logit, 0.0) + jnp.log1p(jnp.exp(-jnp.abs(logit)))
+        log_gate = -speed_ref[0:1, h : h + 1] * softplus + log_ref[h : h + 1, :]
+        beta = 1.0 / (1.0 + jnp.exp(-correct_ref[h : h + 1, :].astype(jnp.float32)))
+        for n in range(count):
+            lrow_s[n] = log_gate[:, n * SPAN : (n + 1) * SPAN]
+            brow_s[n] = beta[:, n * SPAN : (n + 1) * SPAN]
+        ccol = jnp.sum(jnp.where(rows >= cols_at, lrow_s[...], 0.0), axis=2, keepdims=True)
+        ccol_s[h] = ccol
+        crow_s[h] = jnp.sum(jnp.where(rows == cols_at, ccol, 0.0), axis=1, keepdims=True)
+        bcol_s[h] = jnp.sum(
+            jnp.where(rows == cols_at, brow_s[...], 0.0), axis=2, keepdims=True
+        )
 
     for o in range(1, devices):
         peer = (e + o) % devices
@@ -561,6 +612,8 @@
         tot_bf[h] = state.astype(jnp.bfloat16)
         return carry
 
+    for copy in early[1:]:
+        copy.wait()
     lax.fori_loop(0, heads, local_head, 0)
 
     odd = e % 2
@@ -746,8 +799,12 @@
             slot_out.at[e, :, cols(j)], returned.at[e, :, cols(j)], r_local.at[j]
         ).wait()
         back = returned[:, :, j * cut : (j + 1) * cut].reshape(slots, cut)
-        routed = jnp.dot(coarse_ref[...], back, preferred_element_type=jnp.float32) + jnp.dot(
-            fine_ref[...], back, preferred_element_type=jnp.float32
+        routed = sum(
+            weight_ref[n]
+            * lax.dot_general(
+                hits_ref[n], back, (((0,), (0,)), ((), ())), preferred_element_type=jnp.float32
+            )
+            for n in range(top_k)
         )
         moe_ref[:, j * cut : (j + 1) * cut] = (
             shared[:, j * cut : (j + 1) * cut] + routed
@@ -782,6 +839,11 @@
     def _():
         remote(s_out, s_in, c_send.at[1], c_recv.at[1], (next_odd, t)).wait_send()
         remote(s_out, s_in, c_send.at[2], c_recv.at[1], (next_even, t)).wait_send()
+
+
+def hand_over(mixed_ref, routed_ref, mixer_out_ref, moe_out_ref):
+    mixer_out_ref[...] = mixed_ref[...]
+    moe_out_ref[...] = routed_ref[...]
 
 
 def fused_shards(
@@ -816,28 +878,15 @@
     shared_unit = common_gate_weight.shape[1]
     capacity = 3 * tokens * top_k // (2 * devices)
     slot_count = devices * capacity
-    slots = slot_layout(routes, capacity)
-    numbers = jnp.arange(slot_count, dtype=jnp.int32)
-    sends = sum(
-        (slots[None, :, k] == numbers[:, None]).astype(jnp.bfloat16) for k in range(top_k)
-    )
-    weights = sum(
-        jnp.where(
-            slots[:, k : k + 1] == numbers[None, :], chosen_expert_weight[:, k : k + 1], 0.0
-        )
-        for k in range(top_k)
-    )
-    coarse = weights.astype(jnp.bfloat16)
-    fine = (weights - coarse.astype(jnp.float32)).astype(jnp.bfloat16)
     bf, f32 = jnp.bfloat16, jnp.float32
     vmem = pl.BlockSpec(memory_space=pltpu.VMEM)
     anywhere = pl.BlockSpec(memory_space=pl.ANY)
     dma = pltpu.SemaphoreType.DMA
     quarter = (4, tokens, model)
     slot_shape = (devices, capacity, model)
-    return pl.pallas_call(
+    mixed, routed = pl.pallas_call(
         functools.partial(fused_kernel, devices),
-        in_specs=[vmem] * 13 + [anywhere] * 7,
+        in_specs=[vmem] * 8 + [anywhere] * 11,
         out_specs=[vmem, vmem],
         out_shape=[jax.ShapeDtypeStruct((tokens, model), bf)] * 2,
         scratch_shapes=[
@@ -848,6 +897,14 @@
             pltpu.VMEM((model, shared_unit), bf),
             pltpu.VMEM((shared_unit, model), bf),
             pltpu.VMEM(mixer_output_weight.shape, bf),
+            pltpu.VMEM(queries.shape, bf),
+            pltpu.VMEM(queries.shape, bf),
+            pltpu.VMEM(queries.shape, bf),
+            pltpu.VMEM((tokens, model), bf),
+            pltpu.VMEM((top_k, slot_count, tokens), bf),
+            pltpu.VMEM((top_k, tokens, 1), f32),
+            pltpu.VMEM((count, 1, SPAN), f32),
+            pltpu.VMEM((count, 1, SPAN), f32),
             pltpu.VMEM(quarter, bf),
             pltpu.VMEM(slot_shape, bf),
             pltpu.VMEM(slot_shape, bf),
@@ -875,7 +932,7 @@
             pltpu.VMEM((heads, width, width), bf),
             pltpu.VMEM((heads, width, width), f32),
             pltpu.VMEM((length, heads * width), bf),
-            dma((8,)),
+            dma((12,)),
             dma((3 + CUTS, 3)),
             dma((3 + CUTS, 3)),
             dma((devices - 1,)),
@@ -892,19 +949,18 @@
             collective_id=0, has_side_effects=True, vmem_limit_bytes=62 << 20
         ),
     )(
+        decay_gate_logits.T,
+        correction_logits.T,
+        head_decay_speed.reshape(1, heads),
+        position_log_decay.T,
+        head_output_gain.reshape(1, width),
+        expert_norm_gain.reshape(1, model),
+        routes.T,
+        chosen_expert_weight.T,
         queries,
         keys,
         values,
-        decay_gate_logits,
-        correction_logits,
-        head_decay_speed.reshape(1, heads),
-        position_log_decay,
-        head_output_gain.reshape(1, width),
         expert_input_tokens,
-        expert_norm_gain.reshape(1, model),
-        sends,
-        coarse,
-        fine,
         mixer_output_weight,
         routed_gate_weight[0],
         routed_up_weight[0],
@@ -913,6 +969,14 @@
         common_up_weight,
         common_down_weight,
     )
+    half = pl.BlockSpec((tokens // 2, model), lambda n: (n, 0))
+    return pl.pallas_call(
+        hand_over,
+        grid=(2,),
+        in_specs=[half, half],
+        out_specs=[half, half],
+        out_shape=[jax.ShapeDtypeStruct((tokens, model), bf)] * 2,
+    )(mixed, routed)
 
 
 def shards(*args):

time: 129 us -> 117 us (0.907)
  local copies, waits for them, and re-layouts: 10.2 us -> 0 us
  other arithmetic: 2.39 us -> 0 us
    unnamed x6 -> x0, local copies, waits for them, and re-layouts: 9.13 us -> none
    pallas_call x0 -> x1, Pallas kernels: none -> 2.04 us  [fused_shards(): pl.pallas_call(hand_over, grid=(2,), in_specs=[half, half], out_specs=[ha...]
    add x2 -> x0, other arithmetic: 1.39 us -> none  [the longest x1 0.71 us: slot_layout(): return (flat * capacity + before).reshape(routes.shape)]
where the time goes in v1:
time: 117 us
  Pallas kernels  116 us (99%)
    pallas_call x1, Pallas kernels, fused_shards(): pl.pallas_call(functools.partial(fused_kernel, devices), in_specs=[vmem]...  114 us

profile of v1, /device:TPU:0, one launch (start us, length us, event | category | flops | bytes accessed | tf_op | source)
XLA Modules:
  0.0 117.1 jit_solution(15398831727511270818)
XLA Ops:
  0.6 114.4 %shard_map.194 = (bf16[128,2048]{1,0:T(8,128)(2,1)}, bf16[128,2048]{1,0:T(8,128)(2,1)}) custom-call(f32[3,512]{1,0:T(4,128)} %bitcast.14, bf16[3,512]{1,0:T(4,128)(2,1)} %bitcast.17, f32[1,3]{1,0:T(1,128)} %bitcast.20, f32[3,512]{1,0:T(4,128)} %bitcast.15, f32[1,128]{1,0:T(1,128)} %bitcast.21, f32[1,2048]{1,0:T(1,128)} %bitcast.16, s32[2,128]{1,0:T(2,128)} %bitcast.18, ...), custom_call_target="tpu_custom_call" | custom-call | tf_op jit(solution)/shard_map/pallas_call | solution.py:887
  115.0 2.0 %shard_map.195 = (bf16[128,2048]{1,0:T(8,128)(2,1)}, bf16[128,2048]{1,0:T(8,128)(2,1)}) custom-call(bf16[128,2048]{1,0:T(8,128)(2,1)} %get-tuple-element.4.mixed_ref, bf16[128,2048]{1,0:T(8,128)(2,1)} %get-tuple-element.5.routed_ref), custom_call_target="tpu_custom_call" | custom-call | tf_op jit(solution)/shard_map/pallas_call | solution.py:973

commit v2 on v1

--- a/solution.py
+++ b/solution.py
@@ -312,7 +312,7 @@
 
 
 MESH = pl.DeviceIdType.MESH
-CUTS = 4
+CUTS = 8
 OWN, CORE, CROSS, FAR = range(4)
 
 
@@ -354,7 +354,7 @@
     wd,
     cg,
     cu,
-    cd,
+    dn,
     mw,
     q_ref,
     k_ref,
@@ -365,15 +365,14 @@
     lrow_s,
     brow_s,
     toks,
+    sh_hid,
+    sh_in,
     outgoing,
     arrived,
     hid,
     slot_out,
     returned,
-    sh_part,
-    sh_in,
-    sh_cross,
-    sh_far,
+    shared,
     mx_part,
     mx_in,
     mx_cross,
@@ -403,6 +402,22 @@
     rs_recv,
     c_send,
     c_recv,
+    sx_send,
+    sx_recv,
+    sc_send,
+    sc_recv,
+    z_send,
+    z_recv,
+    zf_send,
+    y_send,
+    y_recv,
+    f_send,
+    f_recv,
+    h_send,
+    h_recv,
+    o_sem,
+    mix_s,
+    moe_s,
 ):
     e = lax.axis_index("ep")
     t = lax.axis_index("tp")
@@ -419,6 +434,14 @@
     core_t = t + 1 - 2 * (t % 2)
     core = (e, core_t)
     cross = (e, (t + 2) % 4)
+    line = devices // 2
+    half = line // 2
+    z = e // 2
+    y = e % 2
+    inner = z % half
+    mine = z - inner
+    other = half - mine
+    beside = (2 * z + 1 - y, t)
 
     def remote(src, dst, send, recv, peer):
         return pltpu.make_async_remote_copy(
@@ -430,6 +453,17 @@
             device_id_type=MESH,
         )
 
+    near = [
+        2 * (mine + (inner + o) % half) + (y + d) % 2
+        for o in range(half)
+        for d in range(2)
+        if (o, d) != (0, 0)
+    ]
+    distant = [
+        2 * (other + (inner + o) % half) + (y + d) % 2 for o in range(half) for d in range(2)
+    ]
+    peers = distant + near
+
     early = [
         pltpu.make_async_copy(src, dst, local_sem.at[8 + n])
         for n, (src, dst) in enumerate(
@@ -442,7 +476,7 @@
             (
                 (cg_hbm, cg),
                 (cu_hbm, cu),
-                (cd_hbm, cd),
+                (cd_hbm, dn.at[OWN]),
                 (rg_hbm, wg.at[OWN]),
                 (ru_hbm, wu.at[OWN]),
                 (rd_hbm, wd.at[OWN]),
@@ -510,29 +544,35 @@
         remote(place(CORE), place(CORE), w_send.at[i, 1], w_recv.at[i, 1], core).wait_send()
         remote(place(FAR), place(FAR), w_send.at[i, 2], w_recv.at[i, 2], core).wait_send()
 
+    def gate_at(r):
+        return wg.at[r]
+
+    def up_at(r):
+        return wu.at[r]
+
+    def down_at(j):
+        return lambda r: wd.at[r, :, cols(j)]
+
     def tok_at(r):
         return toks.at[r]
 
-    def gate_at(r):
-        return wg.at[r]
-
-    def up_at(r):
-        return wu.at[r]
-
-    def down_at(j):
-        return lambda r: wd.at[r, :, cols(j)]
-
-    spread(0, tok_hbm, tok_at)
-    spread(1, rg_hbm, gate_at)
-    spread(2, ru_hbm, up_at)
-    for j in range(CUTS):
-        remote(
-            rd_hbm.at[:, cols(j)], wd.at[CROSS, :, cols(j)], w_send.at[3 + j, 0], w_recv.at[3 + j, 0], cross
-        ).start()
-        remote(
-            rd_hbm.at[:, cols(j)], wd.at[CORE, :, cols(j)], w_send.at[3 + j, 1], w_recv.at[3 + j, 1], core
-        ).start()
-
+    slices = [remote(cd_hbm.at[e], dn.at[CROSS, e], sx_send, sx_recv, cross)]
+    for copy in slices:
+        copy.start()
+    spread(0, rg_hbm, gate_at)
+    spread(1, ru_hbm, up_at)
+
+    def spread_down(j, carry):
+        spread(2 + j, rd_hbm.at[:, cols(j)], down_at(j))
+        return carry
+
+    ahead = 5 * CUTS // 8
+    lax.fori_loop(0, ahead, spread_down, 0)
+    spread(2 + CUTS, tok_hbm, tok_at)
+    lax.fori_loop(ahead, CUTS, spread_down, 0)
+    shared_core = [remote(cd_hbm, dn.at[CORE], sc_send, sc_recv, core)]
+    for copy in shared_core:
+        copy.start()
     for copy in locals_:
         copy.start()
 
@@ -561,11 +601,12 @@
             jnp.where(rows == cols_at, brow_s[...], 0.0), axis=2, keepdims=True
         )
 
-    for o in range(1, devices):
-        peer = (e + o) % devices
-        remote(
-            outgoing.at[peer], arrived.at[e], d_send.at[o - 1], d_recv.at[o - 1], (peer, t)
-        ).start()
+    def dispatch(n):
+        peer = peers[n]
+        return remote(outgoing.at[peer], arrived.at[e], d_send.at[n], d_recv.at[n], (peer, t))
+
+    for n in range(len(peers)):
+        dispatch(n).start()
     own_rows = pltpu.make_async_copy(outgoing.at[e], arrived.at[e], local_sem.at[7])
     own_rows.start()
 
@@ -616,86 +657,95 @@
         copy.wait()
     lax.fori_loop(0, heads, local_head, 0)
 
-    odd = e % 2
-    pair = e // 2
-    pairs = devices // 2
-    forward(0, tok_at)
-    to_odd = remote(tot_bf, pair_in, c_send.at[0], c_recv.at[0], ((e + 1) % devices, t))
-
-    @pl.when(odd == 0)
+    def piece(i, r, send, recv, peer):
+        return [remote(dn.at[CROSS, i], dn.at[r, i], send, recv, peer)]
+
+    def along(at, n, place):
+        i = 2 * at + y
+        return piece(i, CROSS, z_send.at[n], z_recv.at[at], (2 * place + y, t))
+
+    def hand_on(o, n, at):
+        place = mine + (inner + o) % half
+        return piece(
+            2 * at + y,
+            CROSS,
+            zf_send.at[(o - 1) * half + n],
+            z_recv.at[at],
+            (2 * place + y, t),
+        )
+
+    def aside(at):
+        return piece(2 * at + y, CROSS, y_send.at[at], y_recv.at[at], beside)
+
+    def to_core(i):
+        return piece(i, FAR, f_send.at[i], f_recv.at[i], core)
+
+    def share(at):
+        for copy in aside(at) + to_core(2 * at + y):
+            copy.start()
+
+    half_places = [mine + (inner + o) % half for o in range(half)]
+    far_places = [other + (inner + o) % half for o in range(half)]
+    middle = half - z // half
+    is_middle = jnp.logical_or(z == half - 1, z == half)
+
+    def line_copies():
+        copies = along(z, 0, middle)
+        for o in range(1, half):
+            copies += along(z, o, half_places[o])
+        return copies
+
+    pair = z
+    to_odd = remote(tot_bf, pair_in, c_send.at[0], c_recv.at[0], beside)
+    next_odd = ((e + 2) % devices, t)
+    next_even = ((e + 1) % devices, t)
+    hands_on = jnp.logical_and(y == 1, pair < line - 1)
+    to_next_odd = remote(s_out, s_in, c_send.at[1], c_recv.at[1], next_odd)
+    to_next_even = remote(s_out, s_in, c_send.at[2], c_recv.at[1], next_even)
+
+    @pl.when(y == 0)
     def _():
         to_odd.start()
 
-    take(0, tok_at)
-    for n in range(3):
-        locals_[n].wait()
-    gain = gain_ref[...]
-    for r in (CORE, CROSS, FAR):
-        if r == CROSS:
-            remote(tok_at(FAR), tok_at(FAR), w_send.at[0, 2], w_recv.at[0, 2], core).wait_send()
-        toks[r] = scaled_rows(toks[r], gain)
-    x_all = toks[...].reshape(4 * tokens, model)
-    sh_hid = silu_product(
-        jnp.dot(x_all, cg[...], preferred_element_type=jnp.float32),
-        jnp.dot(x_all, cu[...], preferred_element_type=jnp.float32),
-    )
-    sh_part[...] = (
-        jnp.dot(sh_hid, cd[...], preferred_element_type=jnp.float32)
-        .astype(jnp.bfloat16)
-        .reshape(sh_part.shape)
-    )
-
-    def reduce_start(n, part, inbox):
-        for i, r in enumerate((FAR, CORE)):
-            remote(
-                part.at[r], inbox.at[1 - i], rs_send.at[n, i], rs_recv.at[n, i], core
-            ).start()
-
-    def reduce_cross(n, part, inbox, out, far):
-        remote(part.at[FAR], inbox.at[1], rs_send.at[n, 0], rs_recv.at[n, 0], core).wait_recv()
-        out[...] = (part[CROSS].astype(jnp.float32) + inbox[1].astype(jnp.float32)).astype(
-            jnp.bfloat16
-        )
-        remote(out, far, rs_send.at[n, 2], rs_recv.at[n, 2], cross).start()
-
-    def reduce_finish(n, part, inbox, out, far):
-        remote(part.at[CORE], inbox.at[0], rs_send.at[n, 1], rs_recv.at[n, 1], core).wait_recv()
-        remote(out, far, rs_send.at[n, 2], rs_recv.at[n, 2], cross).wait_recv()
-        return (
-            part[OWN].astype(jnp.float32)
-            + inbox[0].astype(jnp.float32)
-            + far[...].astype(jnp.float32)
-        )
-
-    def reduce_sent(n, part, inbox, out, far):
-        remote(part.at[FAR], inbox.at[1], rs_send.at[n, 0], rs_recv.at[n, 0], core).wait_send()
-        remote(part.at[CORE], inbox.at[0], rs_send.at[n, 1], rs_recv.at[n, 1], core).wait_send()
-        remote(out, far, rs_send.at[n, 2], rs_recv.at[n, 2], cross).wait_send()
-
-    reduce_start(0, sh_part, sh_in)
-
-    @pl.when(odd == 1)
-    def _():
-        remote(tot_bf, pair_in, c_send.at[0], c_recv.at[0], ((e + 1) % devices, t)).wait_recv()
+    @pl.when(y == 1)
+    def _():
+        to_odd.wait_recv()
         for h in range(heads):
             both = mm(tot[h][:, :width], pair_in[h].astype(jnp.float32))
             pair_tot[h, :, :width] = both[:, :width]
             pair_tot[h, :, width:] = both[:, width:] + tot[h][:, width:]
 
-    reduce_cross(0, sh_part, sh_in, sh_cross, sh_far)
-
-    forward(1, gate_at)
+    @pl.when(pair == 0)
+    def _():
+        s_in[...] = jnp.zeros_like(s_in)
+
+    @pl.when(jnp.logical_and(hands_on, pair == 0))
+    def _():
+        s_out[...] = pair_tot[:, :, width:].astype(jnp.bfloat16)
+        to_next_odd.start()
+        to_next_even.start()
+
+    late = jnp.logical_and(z > 0, z < half)
+    for copy in slices:
+        copy.wait_recv()
+    share(z)
+
+    @pl.when(jnp.logical_not(late))
+    def _():
+        for copy in line_copies():
+            copy.start()
+
+    forward(0, gate_at)
     for n in range(3, 6):
         locals_[n].wait()
-    for i in (1, 2):
+    for i in (0, 1):
         remote(
             wg.at[CORE], wg.at[CORE], w_send.at[i, 1], w_recv.at[i, 1], core
         ).wait_recv()
+
     own_rows.wait()
-    for o in range(1, devices):
-        remote(
-            outgoing.at[e], arrived.at[e], d_send.at[o - 1], d_recv.at[o - 1], (e, core_t)
-        ).wait_recv()
+    for n in range(len(peers)):
+        dispatch(n).wait_recv()
 
     def hidden_of(r, carry):
         rows_in = arrived[...].reshape(slots, model)
@@ -707,34 +757,32 @@
 
     lax.fori_loop(OWN, CORE + 1, hidden_of, 0)
 
-    next_odd = (e + 2) % devices
-    next_even = (e + 1) % devices
-
     @pl.when(pair > 0)
     def _():
-        remote(s_out, s_in, c_send.at[1], c_recv.at[1], (next_odd, t)).wait_recv()
-
-    @pl.when(pair == 0)
-    def _():
-        s_in[...] = jnp.zeros_like(s_in)
-
-    @pl.when(jnp.logical_and(odd == 1, pair < pairs - 1))
+        to_next_odd.wait_recv()
+
+    @pl.when(jnp.logical_and(hands_on, pair > 0))
     def _():
         for h in range(heads):
             s_out[h] = (
                 mm(pair_tot[h][:, :width], s_in[h].astype(jnp.float32)) + pair_tot[h][:, width:]
             ).astype(jnp.bfloat16)
-        remote(s_out, s_in, c_send.at[1], c_recv.at[1], (next_odd, t)).start()
-        remote(s_out, s_in, c_send.at[2], c_recv.at[1], (next_even, t)).start()
-
-    @pl.when(odd == 1)
+        to_next_odd.start()
+        to_next_even.start()
+
+    @pl.when(late)
+    def _():
+        for copy in line_copies():
+            copy.start()
+
+    @pl.when(y == 1)
     def _():
         for h in range(heads):
             state_s[h] = mm(
                 pair_in[h][:, :width].astype(jnp.float32), s_in[h].astype(jnp.float32)
             ) + pair_in[h][:, width:].astype(jnp.float32)
 
-    @pl.when(odd == 0)
+    @pl.when(y == 0)
     def _():
         state_s[...] = s_in[...].astype(jnp.float32)
 
@@ -744,22 +792,58 @@
         normed[:, h * width : (h + 1) * width] = (out * head_gain_ref[...]).astype(jnp.bfloat16)
     locals_[6].wait()
     for r, owner in enumerate((t, core_t, (t + 2) % 4, (core_t + 2) % 4)):
-        mine = pl.ds(pl.multiple_of(owner * tokens, tokens), tokens)
+        block = pl.ds(pl.multiple_of(owner * tokens, tokens), tokens)
         mx_part[r] = jnp.dot(
-            normed[mine, :], mw[...], preferred_element_type=jnp.float32
+            normed[block, :], mw[...], preferred_element_type=jnp.float32
         ).astype(jnp.bfloat16)
-    reduce_start(1, mx_part, mx_in)
-    forward(2, up_at)
-    reduce_cross(1, mx_part, mx_in, mx_cross, mx_far)
-
-    for i in (1, 2):
+    to_peer = [
+        remote(mx_part.at[r], mx_in.at[1 - i], rs_send.at[i], rs_recv.at[i], core)
+        for i, r in enumerate((FAR, CORE))
+    ]
+    for copy in to_peer:
+        copy.start()
+
+    def line_wait(at):
+        for copy in along(at, 0, z):
+            copy.wait_recv()
+
+    for o in range(1, half):
+        line_wait(half_places[o])
+        share(half_places[o])
+
+    @pl.when(is_middle)
+    def _():
+        for n in range(half):
+            line_wait(far_places[n])
+            for o in range(1, half):
+                for copy in hand_on(o, n, far_places[n]):
+                    copy.start()
+            share(far_places[n])
+
+    forward(1, up_at)
+    for i in (0, 1):
         remote(wg.at[FAR], wg.at[FAR], w_send.at[i, 2], w_recv.at[i, 2], core).wait_recv()
     lax.fori_loop(CROSS, FAR + 1, hidden_of, 0)
 
+    def return_of(n, j):
+        peer = peers[n]
+        return remote(
+            slot_out.at[peer, :, cols(j)],
+            returned.at[e, :, cols(j)],
+            r_send.at[j, n],
+            r_recv.at[j, n],
+            (peer, t),
+        )
+
+    def own_return(j):
+        return pltpu.make_async_copy(
+            slot_out.at[e, :, cols(j)], returned.at[e, :, cols(j)], r_local.at[j]
+        )
+
     def down_of(j, carry):
         place = down_at(j)
-        forward(3 + j, place)
-        take(3 + j, place)
+        forward(2 + j, place)
+        take(2 + j, place)
         hidden = jnp.concatenate([hid[r] for r in range(4)], axis=1)
         weight = wd[:, :, cols(j)].reshape(4 * unit, cut)
         slot_out[:, :, cols(j)] = (
@@ -767,38 +851,63 @@
             .astype(jnp.bfloat16)
             .reshape(devices, capacity, cut)
         )
-        for o in range(1, devices):
-            peer = (e + o) % devices
-            remote(
-                slot_out.at[peer, :, cols(j)],
-                returned.at[e, :, cols(j)],
-                r_send.at[j, o - 1],
-                r_recv.at[j, o - 1],
-                (peer, t),
-            ).start()
-        pltpu.make_async_copy(
-            slot_out.at[e, :, cols(j)], returned.at[e, :, cols(j)], r_local.at[j]
-        ).start()
+        for n in range(len(peers)):
+            return_of(n, j).start()
+        own_return(j).start()
         return carry
 
-    lax.fori_loop(0, CUTS, down_of, 0)
-
-    mix_ref[...] = reduce_finish(1, mx_part, mx_in, mx_cross, mx_far).astype(jnp.bfloat16)
-    shared = reduce_finish(0, sh_part, sh_in, sh_cross, sh_far)
-
-    for j in range(CUTS):
-        for o in range(1, devices):
-            remote(
-                slot_out.at[e, :, cols(j)],
-                returned.at[e, :, cols(j)],
-                r_send.at[j, o - 1],
-                r_recv.at[j, o - 1],
-                (e, core_t),
-            ).wait_recv()
-        pltpu.make_async_copy(
-            slot_out.at[e, :, cols(j)], returned.at[e, :, cols(j)], r_local.at[j]
-        ).wait()
-        back = returned[:, :, j * cut : (j + 1) * cut].reshape(slots, cut)
+    lax.fori_loop(0 * CUTS // 8, 2 * CUTS // 8, down_of, 0)
+
+    @pl.when(jnp.logical_not(is_middle))
+    def _():
+        for n in range(half):
+            line_wait(far_places[n])
+            share(far_places[n])
+
+    lax.fori_loop(2 * CUTS // 8, ahead, down_of, 0)
+    forward(2 + CUTS, tok_at)
+    for n in range(2):
+        locals_[n].wait()
+    take(2 + CUTS, tok_at)
+    remote(tok_at(FAR), tok_at(FAR), w_send.at[2 + CUTS, 2], w_recv.at[2 + CUTS, 2], core).wait_send()
+    gain = gain_ref[...]
+    for r in (CORE, CROSS, FAR):
+        toks[r] = scaled_rows(toks[r], gain)
+    x_all = toks[...].reshape(4 * tokens, model)
+    sh_hid[...] = silu_product(
+        jnp.dot(x_all, cg[...], preferred_element_type=jnp.float32),
+        jnp.dot(x_all, cu[...], preferred_element_type=jnp.float32),
+    ).reshape(sh_hid.shape)
+    hidden_out = [
+        remote(sh_hid.at[r], sh_in.at[r], h_send.at[r - 1], h_recv.at[r - 1], peer)
+        for r, peer in ((CORE, core), (CROSS, cross), (FAR, (e, (core_t + 2) % 4)))
+    ]
+    for copy in hidden_out:
+        copy.start()
+
+    to_peer[0].wait_recv()
+    mx_cross[...] = (mx_part[CROSS].astype(jnp.float32) + mx_in[1].astype(jnp.float32)).astype(
+        jnp.bfloat16
+    )
+    over = remote(mx_cross, mx_far, rs_send.at[2], rs_recv.at[2], cross)
+    over.start()
+    for at in range(line):
+        for copy in piece(2 * at + 1 - y, CROSS, y_send.at[at], y_recv.at[at], beside):
+            copy.wait_recv()
+        for copy in to_core(2 * at + 1 - y):
+            copy.start()
+    lax.fori_loop(ahead, CUTS, down_of, 0)
+
+    def moe_out(j):
+        return pltpu.make_async_copy(moe_s.at[:, cols(j)], moe_ref.at[:, cols(j)], o_sem.at[j])
+
+    mix_out = pltpu.make_async_copy(mix_s, mix_ref, local_sem.at[12])
+
+    def combine(j, carry):
+        for n in range(len(peers)):
+            return_of(n, j).wait_recv()
+        own_return(j).wait()
+        back = returned[:, :, cols(j)].reshape(slots, cut)
         routed = sum(
             weight_ref[n]
             * lax.dot_general(
@@ -806,44 +915,92 @@
             )
             for n in range(top_k)
         )
-        moe_ref[:, j * cut : (j + 1) * cut] = (
-            shared[:, j * cut : (j + 1) * cut] + routed
-        ).astype(jnp.bfloat16)
-
-    remote(toks.at[CROSS], toks.at[CROSS], w_send.at[0, 0], w_recv.at[0, 0], cross).wait_send()
-    remote(toks.at[CORE], toks.at[CORE], w_send.at[0, 1], w_recv.at[0, 1], core).wait_send()
-    sent(1, gate_at)
-    sent(2, up_at)
-    for j in range(CUTS):
-        sent(3 + j, down_at(j))
-    for o in range(1, devices):
-        remote(
-            outgoing.at[e], arrived.at[e], d_send.at[o - 1], d_recv.at[o - 1], (e, core_t)
-        ).wait_send()
-        for j in range(CUTS):
-            remote(
-                slot_out.at[e, :, cols(j)],
-                returned.at[e, :, cols(j)],
-                r_send.at[j, o - 1],
-                r_recv.at[j, o - 1],
-                (e, core_t),
-            ).wait_send()
-    reduce_sent(0, sh_part, sh_in, sh_cross, sh_far)
-    reduce_sent(1, mx_part, mx_in, mx_cross, mx_far)
-
-    @pl.when(odd == 0)
+        moe_s[:, cols(j)] = (shared[:, cols(j)] + routed).astype(jnp.bfloat16)
+        moe_out(j).start()
+        return carry
+
+    locals_[2].wait()
+    shared_core[0].wait_recv()
+    for i in range(devices):
+        for copy in to_core(i):
+            copy.wait_recv()
+    for copy in hidden_out:
+        copy.wait_recv()
+    sh_in[OWN] = sh_hid[OWN]
+    shared[...] = jnp.dot(
+        jnp.concatenate([sh_in[r] for r in range(4)], axis=1),
+        dn[...].reshape(4 * dn.shape[1] * dn.shape[2], model),
+        preferred_element_type=jnp.float32,
+    )
+
+    lax.fori_loop(0, CUTS, combine, 0)
+    to_peer[1].wait_recv()
+    over.wait_recv()
+    mix_s[...] = (
+        mx_part[OWN].astype(jnp.float32)
+        + mx_in[0].astype(jnp.float32)
+        + mx_far[...].astype(jnp.float32)
+    ).astype(jnp.bfloat16)
+    mix_out.start()
+    sent(0, gate_at)
+    sent(1, up_at)
+    remote(toks.at[CROSS], toks.at[CROSS], w_send.at[2 + CUTS, 0], w_recv.at[2 + CUTS, 0], cross).wait_send()
+    remote(toks.at[CORE], toks.at[CORE], w_send.at[2 + CUTS, 1], w_recv.at[2 + CUTS, 1], core).wait_send()
+
+    def down_sent(j, carry):
+        sent(2 + j, down_at(j))
+        for n in range(len(peers)):
+            return_of(n, j).wait_send()
+        moe_out(j).wait()
+        return carry
+
+    lax.fori_loop(0, CUTS, down_sent, 0)
+    for n in range(len(peers)):
+        dispatch(n).wait_send()
+    for copy in slices + shared_core + to_peer + line_copies() + hidden_out + [over]:
+        copy.wait_send()
+    for at in range(line):
+        for copy in aside(at):
+            copy.wait_send()
+    for i in range(devices):
+        for copy in to_core(i):
+            copy.wait_send()
+
+    mix_out.wait()
+
+    @pl.when(is_middle)
+    def _():
+        for n in range(half):
+            for o in range(1, half):
+                for copy in hand_on(o, n, far_places[n]):
+                    copy.wait_send()
+
+    @pl.when(y == 0)
     def _():
         to_odd.wait_send()
 
-    @pl.when(jnp.logical_and(odd == 1, pair < pairs - 1))
-    def _():
-        remote(s_out, s_in, c_send.at[1], c_recv.at[1], (next_odd, t)).wait_send()
-        remote(s_out, s_in, c_send.at[2], c_recv.at[1], (next_even, t)).wait_send()
-
-
-def hand_over(mixed_ref, routed_ref, mixer_out_ref, moe_out_ref):
-    mixer_out_ref[...] = mixed_ref[...]
-    moe_out_ref[...] = routed_ref[...]
+    @pl.when(hands_on)
+    def _():
+        to_next_odd.wait_send()
+        to_next_even.wait_send()
+
+
+def hand_over(mixed_hbm, routed_hbm, mixer_out_hbm, moe_out_hbm, held, in_sem, out_sem):
+    pieces, rows = held.shape[0], held.shape[1]
+    each = pieces // 2
+    ins, outs = [], []
+    for n in range(pieces):
+        src, dst = ((mixed_hbm, mixer_out_hbm), (routed_hbm, moe_out_hbm))[n // each]
+        at = pl.ds(n % each * rows, rows)
+        ins.append(pltpu.make_async_copy(src.at[at], held.at[n], in_sem.at[n]))
+        outs.append(pltpu.make_async_copy(held.at[n], dst.at[at], out_sem.at[n]))
+    for copy in ins:
+        copy.start()
+    for taken, given in zip(ins, outs):
+        taken.wait()
+        given.start()
+    for copy in outs:
+        copy.wait()
 
 
 def fused_shards(
@@ -882,20 +1039,21 @@
     vmem = pl.BlockSpec(memory_space=pltpu.VMEM)
     anywhere = pl.BlockSpec(memory_space=pl.ANY)
     dma = pltpu.SemaphoreType.DMA
-    quarter = (4, tokens, model)
+    line = devices // 2
+    half = line // 2
     slot_shape = (devices, capacity, model)
     mixed, routed = pl.pallas_call(
         functools.partial(fused_kernel, devices),
         in_specs=[vmem] * 8 + [anywhere] * 11,
-        out_specs=[vmem, vmem],
+        out_specs=[anywhere, anywhere],
         out_shape=[jax.ShapeDtypeStruct((tokens, model), bf)] * 2,
         scratch_shapes=[
             pltpu.VMEM((4, model, unit), bf),
             pltpu.VMEM((4, model, unit), bf),
             pltpu.VMEM((4, unit, model), bf),
-            pltpu.VMEM((model, shared_unit), bf),
-            pltpu.VMEM((model, shared_unit), bf),
-            pltpu.VMEM((shared_unit, model), bf),
+            pltpu.VMEM(common_gate_weight.shape, bf),
+            pltpu.VMEM(common_up_weight.shape, bf),
+            pltpu.VMEM((4, devices, shared_unit // devices, model), bf),
             pltpu.VMEM(mixer_output_weight.shape, bf),
             pltpu.VMEM(queries.shape, bf),
             pltpu.VMEM(queries.shape, bf),
@@ -905,17 +1063,16 @@
             pltpu.VMEM((top_k, tokens, 1), f32),
             pltpu.VMEM((count, 1, SPAN), f32),
             pltpu.VMEM((count, 1, SPAN), f32),
-            pltpu.VMEM(quarter, bf),
+            pltpu.VMEM((4, tokens, model), bf),
+            pltpu.VMEM((4, tokens, shared_unit), bf),
+            pltpu.VMEM((4, tokens, shared_unit), bf),
             pltpu.VMEM(slot_shape, bf),
             pltpu.VMEM(slot_shape, bf),
             pltpu.VMEM((4, slot_count, unit), bf),
             pltpu.VMEM(slot_shape, bf),
             pltpu.VMEM(slot_shape, bf),
-            pltpu.VMEM(quarter, bf),
-            pltpu.VMEM((2, tokens, model), bf),
-            pltpu.VMEM((tokens, model), bf),
-            pltpu.VMEM((tokens, model), bf),
-            pltpu.VMEM(quarter, bf),
+            pltpu.VMEM((tokens, model), f32),
+            pltpu.VMEM((4, tokens, model), bf),
             pltpu.VMEM((2, tokens, model), bf),
             pltpu.VMEM((tokens, model), bf),
             pltpu.VMEM((tokens, model), bf),
@@ -932,7 +1089,7 @@
             pltpu.VMEM((heads, width, width), bf),
             pltpu.VMEM((heads, width, width), f32),
             pltpu.VMEM((length, heads * width), bf),
-            dma((12,)),
+            dma((13,)),
             dma((3 + CUTS, 3)),
             dma((3 + CUTS, 3)),
             dma((devices - 1,)),
@@ -940,10 +1097,26 @@
             dma((CUTS, devices - 1)),
             dma((CUTS, devices - 1)),
             dma((CUTS,)),
-            dma((2, 3)),
-            dma((2, 3)),
+            dma((3,)),
+            dma((3,)),
             dma((3,)),
             dma((2,)),
+            dma,
+            dma,
+            dma,
+            dma,
+            dma((half,)),
+            dma((line,)),
+            dma((half * half,)),
+            dma((line,)),
+            dma((line,)),
+            dma((devices,)),
+            dma((devices,)),
+            dma((3,)),
+            dma((3,)),
+            dma((CUTS,)),
+            pltpu.VMEM((tokens, model), bf),
+            pltpu.VMEM((tokens, model), bf),
         ],
         compiler_params=pltpu.CompilerParams(
             collective_id=0, has_side_effects=True, vmem_limit_bytes=62 << 20
@@ -967,15 +1140,14 @@
         routed_down_weight[0],
         common_gate_weight,
         common_up_weight,
-        common_down_weight,
-    )
-    half = pl.BlockSpec((tokens // 2, model), lambda n: (n, 0))
+        common_down_weight.reshape(devices, shared_unit // devices, model),
+    )
     return pl.pallas_call(
         hand_over,
-        grid=(2,),
-        in_specs=[half, half],
-        out_specs=[half, half],
+        in_specs=[anywhere] * 2,
+        out_specs=[anywhere] * 2,
         out_shape=[jax.ShapeDtypeStruct((tokens, model), bf)] * 2,
+        scratch_shapes=[pltpu.VMEM((8, tokens // 4, model), bf), dma((8,)), dma((8,))],
     )(mixed, routed)
 
 
@@ -984,7 +1156,9 @@
     routes, tokens = args[11], args[9]
     capacity = 3 * routes.shape[0] * routes.shape[1] // (2 * devices)
     whole_tiles = capacity % 16 == 0 and tokens.shape[1] % (128 * CUTS) == 0
-    if members == 4 and devices % 2 == 0 and whole_tiles:
+    whole_tiles = whole_tiles and args[16].shape[1] % (16 * devices) == 0
+    whole_tiles = whole_tiles and args[16].shape[1] == args[13].shape[2]
+    if members == 4 and devices % 4 == 0 and whole_tiles:
         return fused_shards(*args)
     return plain_shards(*args)
 

time: 117 us -> 111 us (0.949)
  Pallas kernels: 116 us -> 110 us
    pallas_call x1, Pallas kernels: 114 us -> 108 us  [fused_shards(): pl.pallas_call(functools.partial(fused_kernel, devices), in_specs=[vmem]...]
where the time goes in v2:
time: 111 us
  Pallas kernels  110 us (99%)
    pallas_call x1, Pallas kernels, fused_shards(): pl.pallas_call(functools.partial(fused_kernel, devices), in_specs=[vmem]...  108 us

profile of v2, /device:TPU:0, one launch (start us, length us, event | category | flops | bytes accessed | tf_op | source)
XLA Modules:
  0.0 110.8 jit_solution(13855405312939144694)
XLA Ops:
  0.6 107.9 %shard_map.194 = (bf16[128,2048]{1,0:T(8,128)(2,1)}, bf16[128,2048]{1,0:T(8,128)(2,1)}) custom-call(f32[3,512]{1,0:T(4,128)} %bitcast.16, bf16[3,512]{1,0:T(4,128)(2,1)} %bitcast.19, f32[1,3]{1,0:T(1,128)} %bitcast.22, f32[3,512]{1,0:T(4,128)} %bitcast.17, f32[1,128]{1,0:T(1,128)} %bitcast.23, f32[1,2048]{1,0:T(1,128)} %bitcast.18, s32[2,128]{1,0:T(2,128)} %bitcast.20, ...), custom_call_target="tpu_custom_call" | custom-call | tf_op jit(solution)/shard_map/pallas_call | solution.py:1045
  108.5 2.1 %shard_map.195 = (bf16[128,2048]{1,0:T(8,128)(2,1)}, bf16[128,2048]{1,0:T(8,128)(2,1)}) custom-call(bf16[128,2048]{1,0:T(8,128)(2,1)} %get-tuple-element.4.mixed_hbm, bf16[128,2048]{1,0:T(8,128)(2,1)} %get-tuple-element.5.routed_hbm), custom_call_target="tpu_custom_call" | custom-call | tf_op jit(solution)/shard_map/pallas_call | solution.py:1145

commit v3 on v2

--- a/solution.py
+++ b/solution.py
@@ -393,11 +393,12 @@
     local_sem,
     w_send,
     w_recv,
+    p_recv,
+    g_recv,
     d_send,
     d_recv,
     r_send,
     r_recv,
-    r_local,
     rs_send,
     rs_recv,
     c_send,
@@ -416,6 +417,8 @@
     h_send,
     h_recv,
     o_sem,
+    here_sem,
+    go_sem,
     mix_s,
     moe_s,
 ):
@@ -488,12 +491,13 @@
         copy.start()
 
     barrier = pltpu.get_barrier_semaphore()
-    for o in range(1, devices):
-        pl.semaphore_signal(
-            barrier, inc=1, device_id=((e + o) % devices, t), device_id_type=MESH
-        )
+    speaker = t == 3
     for o in range(1, 4):
-        pl.semaphore_signal(barrier, inc=1, device_id=(e, (t + o) % 4), device_id_type=MESH)
+        member = (t + o) % 4
+
+        @pl.when(member != 3)
+        def _():
+            pl.semaphore_signal(barrier, inc=1, device_id=(e, member), device_id_type=MESH)
 
     expert = lax.broadcasted_iota(jnp.int32, (devices, tokens), 0)
     earlier = lax.broadcasted_iota(jnp.int32, (tokens, tokens), 0)
@@ -522,53 +526,64 @@
             jnp.where(token_a == token_b, chosen_ref[n : n + 1, :], 0.0), axis=1, keepdims=True
         )
 
-    pl.semaphore_wait(barrier, devices + 2)
+    @pl.when(jnp.logical_not(speaker))
+    def _():
+        pl.semaphore_wait(barrier, 3)
+        pl.semaphore_signal(here_sem, inc=1, device_id=(e, 3), device_id_type=MESH)
+
+    @pl.when(speaker)
+    def _():
+        pl.semaphore_wait(here_sem, 3)
+        for o in range(1, devices):
+            pl.semaphore_signal(
+                barrier, inc=1, device_id=((e + o) % devices, t), device_id_type=MESH
+            )
+
 
     def cols(j):
         return pl.ds(pl.multiple_of(j * cut, cut), cut)
 
-    def spread(i, src, place):
-        remote(src, place(CROSS), w_send.at[i, 0], w_recv.at[i, 0], cross).start()
-        remote(src, place(CORE), w_send.at[i, 1], w_recv.at[i, 1], core).start()
-
-    def forward(i, place):
-        remote(place(CROSS), place(CROSS), w_send.at[i, 0], w_recv.at[i, 0], cross).wait_recv()
-        remote(place(CROSS), place(FAR), w_send.at[i, 2], w_recv.at[i, 2], core).start()
-
-    def take(i, place):
-        remote(place(CORE), place(CORE), w_send.at[i, 1], w_recv.at[i, 1], core).wait_recv()
-        remote(place(FAR), place(FAR), w_send.at[i, 2], w_recv.at[i, 2], core).wait_recv()
-
-    def sent(i, place):
-        remote(place(CROSS), place(CROSS), w_send.at[i, 0], w_recv.at[i, 0], cross).wait_send()
-        remote(place(CORE), place(CORE), w_send.at[i, 1], w_recv.at[i, 1], core).wait_send()
-        remote(place(FAR), place(FAR), w_send.at[i, 2], w_recv.at[i, 2], core).wait_send()
+    def spread(n, i, src, place):
+        remote(src, place(CROSS), w_send.at[n], w_recv.at[i], cross).start()
+        remote(src, place(CORE), w_send.at[n], p_recv.at[i], core).start()
+
+    def forward(n, i, place):
+        remote(place(CROSS), place(CROSS), w_send.at[n], w_recv.at[i], cross).wait_recv()
+        remote(place(CROSS), place(FAR), w_send.at[n], p_recv.at[i], core).start()
+
+    def take(i, both):
+        remote(both, both, w_send.at[0], p_recv.at[i], core).wait_recv()
+
+    def sent(n, all_of):
+        remote(all_of, all_of, w_send.at[n], w_recv.at[0], core).wait_send()
 
     def gate_at(r):
         return wg.at[r]
 
-    def up_at(r):
-        return wu.at[r]
-
     def down_at(j):
         return lambda r: wd.at[r, :, cols(j)]
-
-    def tok_at(r):
-        return toks.at[r]
 
     slices = [remote(cd_hbm.at[e], dn.at[CROSS, e], sx_send, sx_recv, cross)]
     for copy in slices:
         copy.start()
-    spread(0, rg_hbm, gate_at)
-    spread(1, ru_hbm, up_at)
+    spread(0, 0, rg_hbm, gate_at)
+    hu = unit // 2
+    up_index = (1, 3 + CUTS)
+    for n in range(2):
+        at = pl.ds(n * hu, hu)
+        remote(
+            ru_hbm.at[:, at], wu.at[CROSS, :, at], w_send.at[1], w_recv.at[up_index[n]], cross
+        ).start()
+    remote(ru_hbm, wu.at[CORE], w_send.at[1], p_recv.at[1], core).start()
 
     def spread_down(j, carry):
-        spread(2 + j, rd_hbm.at[:, cols(j)], down_at(j))
+        spread(2, 2 + j, rd_hbm.at[:, cols(j)], down_at(j))
         return carry
 
     ahead = 5 * CUTS // 8
     lax.fori_loop(0, ahead, spread_down, 0)
-    spread(2 + CUTS, tok_hbm, tok_at)
+    remote(tok_hbm, toks.at[CROSS], w_send.at[3], w_recv.at[2 + CUTS], cross).start()
+    remote(tok_hbm, toks.at[CORE], w_send.at[3], p_recv.at[2 + CUTS], core).start()
     lax.fori_loop(ahead, CUTS, spread_down, 0)
     shared_core = [remote(cd_hbm, dn.at[CORE], sc_send, sc_recv, core)]
     for copy in shared_core:
@@ -603,11 +618,21 @@
 
     def dispatch(n):
         peer = peers[n]
-        return remote(outgoing.at[peer], arrived.at[e], d_send.at[n], d_recv.at[n], (peer, t))
+        return remote(outgoing.at[peer], arrived.at[e], d_send, d_recv, (peer, t))
+
+    @pl.when(speaker)
+    def _():
+        pl.semaphore_wait(barrier, devices - 1)
+        for o in range(3):
+            pl.semaphore_signal(go_sem, inc=1, device_id=(e, o), device_id_type=MESH)
+
+    @pl.when(jnp.logical_not(speaker))
+    def _():
+        pl.semaphore_wait(go_sem, 1)
 
     for n in range(len(peers)):
         dispatch(n).start()
-    own_rows = pltpu.make_async_copy(outgoing.at[e], arrived.at[e], local_sem.at[7])
+    own_rows = pltpu.make_async_copy(outgoing.at[e], arrived.at[e], d_recv)
     own_rows.start()
 
     def local_head(h, carry):
@@ -660,25 +685,25 @@
     def piece(i, r, send, recv, peer):
         return [remote(dn.at[CROSS, i], dn.at[r, i], send, recv, peer)]
 
-    def along(at, n, place):
+    def along(at, place):
         i = 2 * at + y
-        return piece(i, CROSS, z_send.at[n], z_recv.at[at], (2 * place + y, t))
-
-    def hand_on(o, n, at):
+        return piece(i, CROSS, z_send, z_recv.at[at], (2 * place + y, t))
+
+    def hand_on(o, at):
         place = mine + (inner + o) % half
         return piece(
             2 * at + y,
             CROSS,
-            zf_send.at[(o - 1) * half + n],
+            zf_send,
             z_recv.at[at],
             (2 * place + y, t),
         )
 
     def aside(at):
-        return piece(2 * at + y, CROSS, y_send.at[at], y_recv.at[at], beside)
+        return piece(2 * at + y, CROSS, y_send, y_recv.at[at], beside)
 
     def to_core(i):
-        return piece(i, FAR, f_send.at[i], f_recv.at[i], core)
+        return piece(i, FAR, f_send, f_recv, core)
 
     def share(at):
         for copy in aside(at) + to_core(2 * at + y):
@@ -690,9 +715,9 @@
     is_middle = jnp.logical_or(z == half - 1, z == half)
 
     def line_copies():
-        copies = along(z, 0, middle)
+        copies = along(z, middle)
         for o in range(1, half):
-            copies += along(z, o, half_places[o])
+            copies += along(z, half_places[o])
         return copies
 
     pair = z
@@ -725,27 +750,21 @@
         to_next_odd.start()
         to_next_even.start()
 
-    late = jnp.logical_and(z > 0, z < half)
     for copy in slices:
         copy.wait_recv()
     share(z)
 
-    @pl.when(jnp.logical_not(late))
-    def _():
-        for copy in line_copies():
-            copy.start()
-
-    forward(0, gate_at)
+    for copy in line_copies():
+        copy.start()
+
+    remote(wg.at[CROSS], wg.at[CROSS], w_send.at[0], w_recv.at[0], cross).wait_recv()
+    remote(wg.at[CROSS], wg.at[FAR], w_send.at[0], g_recv.at[0], core).start()
     for n in range(3, 6):
         locals_[n].wait()
-    for i in (0, 1):
-        remote(
-            wg.at[CORE], wg.at[CORE], w_send.at[i, 1], w_recv.at[i, 1], core
-        ).wait_recv()
-
-    own_rows.wait()
-    for n in range(len(peers)):
-        dispatch(n).wait_recv()
+    take(0, wg.at[CORE])
+    take(1, wu.at[CORE])
+
+    remote(arrived, arrived, d_send, d_recv, core).wait_recv()
 
     def hidden_of(r, carry):
         rows_in = arrived[...].reshape(slots, model)
@@ -757,12 +776,37 @@
 
     lax.fori_loop(OWN, CORE + 1, hidden_of, 0)
 
-    @pl.when(pair > 0)
+    def hidden_half(n):
+        at = slice(n * hu, (n + 1) * hu)
+        rows_in = arrived[...].reshape(slots, model)
+        value = silu_product(
+            *(
+                jnp.dot(
+                    rows_in,
+                    jnp.concatenate([bank[CROSS, :, at], bank[FAR, :, at]], axis=1),
+                    preferred_element_type=jnp.float32,
+                )
+                for bank in (wg, wu)
+            )
+        )
+        hid[CROSS, :, at] = value[:, :hu]
+        hid[FAR, :, at] = value[:, hu:]
+
+    def far_half(n):
+        at = pl.ds(n * hu, hu)
+        there, here = wu.at[CROSS, :, at], wu.at[FAR, :, at]
+        remote(there, there, w_send.at[1], w_recv.at[up_index[n]], cross).wait_recv()
+        remote(there, here, w_send.at[1], g_recv.at[1 + n], core).start()
+        if n == 0:
+            remote(wg.at[FAR], wg.at[FAR], w_send.at[0], g_recv.at[0], core).wait_recv()
+        remote(here, here, w_send.at[1], g_recv.at[1 + n], core).wait_recv()
+        hidden_half(n)
+
+    far_half(0)
+
+    @pl.when(jnp.logical_and(hands_on, pair > 0))
     def _():
         to_next_odd.wait_recv()
-
-    @pl.when(jnp.logical_and(hands_on, pair > 0))
-    def _():
         for h in range(heads):
             s_out[h] = (
                 mm(pair_tot[h][:, :width], s_in[h].astype(jnp.float32)) + pair_tot[h][:, width:]
@@ -770,10 +814,62 @@
         to_next_odd.start()
         to_next_even.start()
 
-    @pl.when(late)
-    def _():
-        for copy in line_copies():
-            copy.start()
+    def line_wait(at):
+        for copy in along(at, z):
+            copy.wait_recv()
+
+    for o in range(1, half):
+        line_wait(half_places[o])
+        share(half_places[o])
+
+    @pl.when(is_middle)
+    def _():
+        for n in range(half):
+            line_wait(far_places[n])
+            for o in range(1, half):
+                for copy in hand_on(o, far_places[n]):
+                    copy.start()
+            share(far_places[n])
+
+    far_half(1)
+
+    def return_of(n, j):
+        peer = peers[n]
+        return remote(
+            slot_out.at[peer, :, cols(j)],
+            returned.at[e, :, cols(j)],
+            r_send,
+            r_recv.at[j],
+            (peer, t),
+        )
+
+    def own_return(j):
+        return pltpu.make_async_copy(
+            slot_out.at[e, :, cols(j)], returned.at[e, :, cols(j)], r_recv.at[j]
+        )
+
+    def down_of(j, carry):
+        place = down_at(j)
+        forward(2, 2 + j, place)
+        take(2 + j, wd.at[pl.ds(0, 2), :, cols(j)])
+        hidden = jnp.concatenate([hid[r] for r in range(4)], axis=1)
+        weight = wd[:, :, cols(j)].reshape(4 * unit, cut)
+        slot_out[:, :, cols(j)] = (
+            jnp.dot(hidden, weight, preferred_element_type=jnp.float32)
+            .astype(jnp.bfloat16)
+            .reshape(devices, capacity, cut)
+        )
+        for n in range(len(peers)):
+            return_of(n, j).start()
+        own_return(j).start()
+        return carry
+
+    lax.fori_loop(0 * CUTS // 8, 2 * CUTS // 8, down_of, 0)
+    lax.fori_loop(2 * CUTS // 8, ahead, down_of, 0)
+
+    @pl.when(jnp.logical_and(jnp.logical_not(hands_on), pair > 0))
+    def _():
+        to_next_odd.wait_recv()
 
     @pl.when(y == 1)
     def _():
@@ -803,73 +899,19 @@
     for copy in to_peer:
         copy.start()
 
-    def line_wait(at):
-        for copy in along(at, 0, z):
-            copy.wait_recv()
-
-    for o in range(1, half):
-        line_wait(half_places[o])
-        share(half_places[o])
-
-    @pl.when(is_middle)
-    def _():
-        for n in range(half):
-            line_wait(far_places[n])
-            for o in range(1, half):
-                for copy in hand_on(o, n, far_places[n]):
-                    copy.start()
-            share(far_places[n])
-
-    forward(1, up_at)
-    for i in (0, 1):
-        remote(wg.at[FAR], wg.at[FAR], w_send.at[i, 2], w_recv.at[i, 2], core).wait_recv()
-    lax.fori_loop(CROSS, FAR + 1, hidden_of, 0)
-
-    def return_of(n, j):
-        peer = peers[n]
-        return remote(
-            slot_out.at[peer, :, cols(j)],
-            returned.at[e, :, cols(j)],
-            r_send.at[j, n],
-            r_recv.at[j, n],
-            (peer, t),
-        )
-
-    def own_return(j):
-        return pltpu.make_async_copy(
-            slot_out.at[e, :, cols(j)], returned.at[e, :, cols(j)], r_local.at[j]
-        )
-
-    def down_of(j, carry):
-        place = down_at(j)
-        forward(2 + j, place)
-        take(2 + j, place)
-        hidden = jnp.concatenate([hid[r] for r in range(4)], axis=1)
-        weight = wd[:, :, cols(j)].reshape(4 * unit, cut)
-        slot_out[:, :, cols(j)] = (
-            jnp.dot(hidden, weight, preferred_element_type=jnp.float32)
-            .astype(jnp.bfloat16)
-            .reshape(devices, capacity, cut)
-        )
-        for n in range(len(peers)):
-            return_of(n, j).start()
-        own_return(j).start()
-        return carry
-
-    lax.fori_loop(0 * CUTS // 8, 2 * CUTS // 8, down_of, 0)
-
     @pl.when(jnp.logical_not(is_middle))
     def _():
         for n in range(half):
             line_wait(far_places[n])
             share(far_places[n])
 
-    lax.fori_loop(2 * CUTS // 8, ahead, down_of, 0)
-    forward(2 + CUTS, tok_at)
+    remote(tok_hbm, toks.at[CROSS], w_send.at[3], w_recv.at[2 + CUTS], cross).wait_recv()
+    toks_on = remote(toks.at[CROSS], toks.at[FAR], w_send.at[4], p_recv.at[2 + CUTS], core)
+    toks_on.start()
     for n in range(2):
         locals_[n].wait()
-    take(2 + CUTS, tok_at)
-    remote(tok_at(FAR), tok_at(FAR), w_send.at[2 + CUTS, 2], w_recv.at[2 + CUTS, 2], core).wait_send()
+    take(2 + CUTS, toks.at[pl.ds(0, 2)])
+    toks_on.wait_send()
     gain = gain_ref[...]
     for r in (CORE, CROSS, FAR):
         toks[r] = scaled_rows(toks[r], gain)
@@ -879,7 +921,7 @@
         jnp.dot(x_all, cu[...], preferred_element_type=jnp.float32),
     ).reshape(sh_hid.shape)
     hidden_out = [
-        remote(sh_hid.at[r], sh_in.at[r], h_send.at[r - 1], h_recv.at[r - 1], peer)
+        remote(sh_hid.at[r], sh_in.at[r], h_send, h_recv, peer)
         for r, peer in ((CORE, core), (CROSS, cross), (FAR, (e, (core_t + 2) % 4)))
     ]
     for copy in hidden_out:
@@ -892,21 +934,20 @@
     over = remote(mx_cross, mx_far, rs_send.at[2], rs_recv.at[2], cross)
     over.start()
     for at in range(line):
-        for copy in piece(2 * at + 1 - y, CROSS, y_send.at[at], y_recv.at[at], beside):
+        for copy in piece(2 * at + 1 - y, CROSS, y_send, y_recv.at[at], beside):
             copy.wait_recv()
         for copy in to_core(2 * at + 1 - y):
             copy.start()
     lax.fori_loop(ahead, CUTS, down_of, 0)
 
     def moe_out(j):
-        return pltpu.make_async_copy(moe_s.at[:, cols(j)], moe_ref.at[:, cols(j)], o_sem.at[j])
+        return pltpu.make_async_copy(moe_s.at[:, cols(j)], moe_ref.at[:, cols(j)], o_sem)
 
     mix_out = pltpu.make_async_copy(mix_s, mix_ref, local_sem.at[12])
 
     def combine(j, carry):
-        for n in range(len(peers)):
-            return_of(n, j).wait_recv()
-        own_return(j).wait()
+        whole = returned.at[:, :, cols(j)]
+        remote(whole, whole, r_send, r_recv.at[j], core).wait_recv()
         back = returned[:, :, cols(j)].reshape(slots, cut)
         routed = sum(
             weight_ref[n]
@@ -921,11 +962,9 @@
 
     locals_[2].wait()
     shared_core[0].wait_recv()
-    for i in range(devices):
-        for copy in to_core(i):
-            copy.wait_recv()
-    for copy in hidden_out:
-        copy.wait_recv()
+    remote(dn.at[FAR], dn.at[FAR], f_send, f_recv, core).wait_recv()
+    others = sh_in.at[pl.ds(CORE, 3)]
+    remote(others, others, h_send, h_recv, core).wait_recv()
     sh_in[OWN] = sh_hid[OWN]
     shared[...] = jnp.dot(
         jnp.concatenate([sh_in[r] for r in range(4)], axis=1),
@@ -942,38 +981,28 @@
         + mx_far[...].astype(jnp.float32)
     ).astype(jnp.bfloat16)
     mix_out.start()
-    sent(0, gate_at)
-    sent(1, up_at)
-    remote(toks.at[CROSS], toks.at[CROSS], w_send.at[2 + CUTS, 0], w_recv.at[2 + CUTS, 0], cross).wait_send()
-    remote(toks.at[CORE], toks.at[CORE], w_send.at[2 + CUTS, 1], w_recv.at[2 + CUTS, 1], core).wait_send()
-
-    def down_sent(j, carry):
-        sent(2 + j, down_at(j))
-        for n in range(len(peers)):
-            return_of(n, j).wait_send()
-        moe_out(j).wait()
-        return carry
-
-    lax.fori_loop(0, CUTS, down_sent, 0)
-    for n in range(len(peers)):
-        dispatch(n).wait_send()
-    for copy in slices + shared_core + to_peer + line_copies() + hidden_out + [over]:
+
+    def gone(all_of, semaphore):
+        remote(all_of, all_of, semaphore, d_recv, core).wait_send()
+
+    sent(0, wg.at[pl.ds(0, 3)])
+    sent(1, wu.at[pl.ds(0, 3)])
+    sent(2, wd.at[pl.ds(0, 3)])
+    sent(3, toks.at[pl.ds(0, 2)])
+    gone(arrived.at[pl.ds(1, devices - 1)], d_send)
+    gone(slot_out.at[pl.ds(1, devices - 1)], r_send)
+    gone(dn.at[FAR, pl.ds(0, half)], z_send)
+    gone(dn.at[FAR, pl.ds(0, line)], y_send)
+    gone(dn.at[FAR], f_send)
+    gone(sh_in.at[pl.ds(CORE, 3)], h_send)
+    for copy in slices + shared_core + to_peer + [over]:
         copy.wait_send()
-    for at in range(line):
-        for copy in aside(at):
-            copy.wait_send()
-    for i in range(devices):
-        for copy in to_core(i):
-            copy.wait_send()
-
+    pltpu.make_async_copy(moe_s, moe_ref, o_sem).wait()
     mix_out.wait()
 
     @pl.when(is_middle)
     def _():
-        for n in range(half):
-            for o in range(1, half):
-                for copy in hand_on(o, n, far_places[n]):
-                    copy.wait_send()
+        gone(dn.at[FAR, pl.ds(0, half * (half - 1))], zf_send)
 
     @pl.when(y == 0)
     def _():
@@ -1040,7 +1069,6 @@
     anywhere = pl.BlockSpec(memory_space=pl.ANY)
     dma = pltpu.SemaphoreType.DMA
     line = devices // 2
-    half = line // 2
     slot_shape = (devices, capacity, model)
     mixed, routed = pl.pallas_call(
         functools.partial(fused_kernel, devices),
@@ -1090,12 +1118,13 @@
             pltpu.VMEM((heads, width, width), f32),
             pltpu.VMEM((length, heads * width), bf),
             dma((13,)),
-            dma((3 + CUTS, 3)),
-            dma((3 + CUTS, 3)),
-            dma((devices - 1,)),
-            dma((devices - 1,)),
-            dma((CUTS, devices - 1)),
-            dma((CUTS, devices - 1)),
+            dma((5,)),
+            dma((4 + CUTS,)),
+            dma((3 + CUTS,)),
+            dma((3,)),
+            dma,
+            dma,
+            dma,
             dma((CUTS,)),
             dma((3,)),
             dma((3,)),
@@ -1105,16 +1134,18 @@
             dma,
             dma,
             dma,
-            dma((half,)),
+            dma,
             dma((line,)),
-            dma((half * half,)),
+            dma,
+            dma,
             dma((line,)),
-            dma((line,)),
-            dma((devices,)),
-            dma((devices,)),
-            dma((3,)),
-            dma((3,)),
-            dma((CUTS,)),
+            dma,
+            dma,
+            dma,
+            dma,
+            dma,
+            pltpu.SemaphoreType.REGULAR,
+            pltpu.SemaphoreType.REGULAR,
             pltpu.VMEM((tokens, model), bf),
             pltpu.VMEM((tokens, model), bf),
         ],
@@ -1158,6 +1189,7 @@
     whole_tiles = capacity % 16 == 0 and tokens.shape[1] % (128 * CUTS) == 0
     whole_tiles = whole_tiles and args[16].shape[1] % (16 * devices) == 0
     whole_tiles = whole_tiles and args[16].shape[1] == args[13].shape[2]
+    whole_tiles = whole_tiles and args[13].shape[2] % 256 == 0
     if members == 4 and devices % 4 == 0 and whole_tiles:
         return fused_shards(*args)
     return plain_shards(*args)

time: 111 us -> 107 us (0.964)
  Pallas kernels: 110 us -> 106 us
    pallas_call x1, Pallas kernels: 108 us -> 104 us  [fused_shards(): pl.pallas_call(functools.partial(fused_kernel, devices), in_specs=[vmem]...]
where the time goes in v3:
time: 107 us
  Pallas kernels  106 us (99%)
    pallas_call x1, Pallas kernels, fused_shards(): pl.pallas_call(functools.partial(fused_kernel, devices), in_specs=[vmem]...  104 us

profile of v3, /device:TPU:0, one launch (start us, length us, event | category | flops | bytes accessed | tf_op | source)
XLA Modules:
  0.0 106.9 jit_solution(12147699520181765749)
XLA Ops:
  0.6 104.0 %shard_map.194 = (bf16[128,2048]{1,0:T(8,128)(2,1)}, bf16[128,2048]{1,0:T(8,128)(2,1)}) custom-call(f32[3,512]{1,0:T(4,128)} %bitcast.16, bf16[3,512]{1,0:T(4,128)(2,1)} %bitcast.19, f32[1,3]{1,0:T(1,128)} %bitcast.22, f32[3,512]{1,0:T(4,128)} %bitcast.17, f32[1,128]{1,0:T(1,128)} %bitcast.23, f32[1,2048]{1,0:T(1,128)} %bitcast.18, s32[2,128]{1,0:T(2,128)} %bitcast.20, ...), custom_call_target="tpu_custom_call" | custom-call | tf_op jit(solution)/shard_map/pallas_call | solution.py:1073
  104.7 2.1 %shard_map.195 = (bf16[128,2048]{1,0:T(8,128)(2,1)}, bf16[128,2048]{1,0:T(8,128)(2,1)}) custom-call(bf16[128,2048]{1,0:T(8,128)(2,1)} %get-tuple-element.4.mixed_hbm, bf16[128,2048]{1,0:T(8,128)(2,1)} %get-tuple-element.5.routed_hbm), custom_call_target="tpu_custom_call" | custom-call | tf_op jit(solution)/shard_map/pallas_call | solution.py:1176

commit v4 on v3

--- a/solution.py
+++ b/solution.py
@@ -328,14 +328,14 @@
 
 def fused_kernel(
     devices,
-    decay_ref,
-    correct_ref,
-    speed_ref,
-    log_ref,
-    head_gain_ref,
-    gain_ref,
-    routes_ref,
-    chosen_ref,
+    decay_hbm,
+    correct_hbm,
+    speed_hbm,
+    log_hbm,
+    head_gain_hbm,
+    gain_hbm,
+    routes_hbm,
+    chosen_hbm,
     q_hbm,
     k_hbm,
     v_hbm,
@@ -364,6 +364,15 @@
     weight_ref,
     lrow_s,
     brow_s,
+    decay_ref,
+    correct_ref,
+    speed_ref,
+    log_ref,
+    head_gain_ref,
+    gain_ref,
+    routes_ref,
+    chosen_ref,
+    thin_sem,
     toks,
     sh_hid,
     sh_in,
@@ -487,8 +496,21 @@
             )
         )
     ]
-    for copy in early:
-        copy.start()
+    thin = [
+        pltpu.make_async_copy(src, dst, thin_sem.at[n])
+        for n, (src, dst) in enumerate(
+            (
+                (routes_hbm, routes_ref),
+                (chosen_hbm, chosen_ref),
+                (gain_hbm, gain_ref),
+                (decay_hbm, decay_ref),
+                (correct_hbm, correct_ref),
+                (speed_hbm, speed_ref),
+                (log_hbm, log_ref),
+                (head_gain_hbm, head_gain_ref),
+            )
+        )
+    ]
 
     barrier = pltpu.get_barrier_semaphore()
     speaker = t == 3
@@ -498,6 +520,11 @@
         @pl.when(member != 3)
         def _():
             pl.semaphore_signal(barrier, inc=1, device_id=(e, member), device_id_type=MESH)
+
+    for copy in thin + early:
+        copy.start()
+    for copy in thin:
+        copy.wait()
 
     expert = lax.broadcasted_iota(jnp.int32, (devices, tokens), 0)
     earlier = lax.broadcasted_iota(jnp.int32, (tokens, tokens), 0)
@@ -1065,14 +1092,13 @@
     capacity = 3 * tokens * top_k // (2 * devices)
     slot_count = devices * capacity
     bf, f32 = jnp.bfloat16, jnp.float32
-    vmem = pl.BlockSpec(memory_space=pltpu.VMEM)
     anywhere = pl.BlockSpec(memory_space=pl.ANY)
     dma = pltpu.SemaphoreType.DMA
     line = devices // 2
     slot_shape = (devices, capacity, model)
     mixed, routed = pl.pallas_call(
         functools.partial(fused_kernel, devices),
-        in_specs=[vmem] * 8 + [anywhere] * 11,
+        in_specs=[anywhere] * 19,
         out_specs=[anywhere, anywhere],
         out_shape=[jax.ShapeDtypeStruct((tokens, model), bf)] * 2,
         scratch_shapes=[
@@ -1091,6 +1117,15 @@
             pltpu.VMEM((top_k, tokens, 1), f32),
             pltpu.VMEM((count, 1, SPAN), f32),
             pltpu.VMEM((count, 1, SPAN), f32),
+            pltpu.VMEM((heads, length), f32),
+            pltpu.VMEM((heads, length), correction_logits.dtype),
+            pltpu.VMEM((1, heads), f32),
+            pltpu.VMEM((heads, length), f32),
+            pltpu.VMEM((1, width), f32),
+            pltpu.VMEM((1, model), f32),
+            pltpu.VMEM((top_k, tokens), routes.dtype),
+            pltpu.VMEM((top_k, tokens), f32),
+            dma((8,)),
             pltpu.VMEM((4, tokens, model), bf),
             pltpu.VMEM((4, tokens, shared_unit), bf),
             pltpu.VMEM((4, tokens, shared_unit), bf),

time: 107 us -> 107 us (level)
  no operation moved by 1% of the time
where the time goes in v4:
time: 107 us; the launch traced here: 106 us
  Pallas kernels  106 us (99%)
    pallas_call x1, Pallas kernels, fused_shards(): pl.pallas_call(functools.partial(fused_kernel, devices), in_specs=[anywhe...  104 us

profile of v4, /device:TPU:0, one launch (start us, length us, event | category | flops | bytes accessed | tf_op | source)
XLA Modules:
  0.0 106.4 jit_solution(16962709514314079209)
XLA Ops:
  0.6 103.5 %shard_map.194 = (bf16[128,2048]{1,0:T(8,128)(2,1)}, bf16[128,2048]{1,0:T(8,128)(2,1)}) custom-call(f32[3,512]{1,0:T(4,128)} %bitcast.16, bf16[3,512]{1,0:T(4,128)(2,1)} %bitcast.19, f32[1,3]{1,0:T(1,128)} %bitcast.22, f32[3,512]{1,0:T(4,128)} %bitcast.17, f32[1,128]{1,0:T(1,128)} %bitcast.23, f32[1,2048]{1,0:T(1,128)} %bitcast.18, s32[2,128]{1,0:T(2,128)} %bitcast.20, ...), custom_call_target="tpu_custom_call" | custom-call | tf_op jit(solution)/shard_map/pallas_call | solution.py:1099
  104.2 2.1 %shard_map.195 = (bf16[128,2048]{1,0:T(8,128)(2,1)}, bf16[128,2048]{1,0:T(8,128)(2,1)}) custom-call(bf16[128,2048]{1,0:T(8,128)(2,1)} %get-tuple-element.4.mixed_hbm, bf16[128,2048]{1,0:T(8,128)(2,1)} %get-tuple-element.5.routed_hbm), custom_call_target="tpu_custom_call" | custom-call | tf_op jit(solution)/shard_map/pallas_call | solution.py:1211
